TPU v7x, 256 devices: a whole 4x4x8 slice. The times are simulated.
256 devices in a mesh: kv: 32 (over z, y), tp: 8 (over x, core).
Axes of the slice: x: 4, y: 4, z: 8, core: 2. Of those that a mesh axis runs over, the one named last changes fastest.
Arguments:
- hidden_rows: bfloat16 [512, 4096], P('kv', 'tp'), may hold values from -16 to 16
- carried_state: float32 [512, 524288], P('kv', 'tp'), may hold values from -6 to 6
- norm_gain: bfloat16 [4096], replicated, may hold values from 0.099609375 to 1.8984375
- w_query: bfloat16 [4096, 2048], P('kv', 'tp'), may hold values from -0.09375 to 0.09375
- w_key: bfloat16 [4096, 2048], P('kv', 'tp'), may hold values from -0.09375 to 0.09375
- w_decay: bfloat16 [4096, 2048], P('kv', 'tp'), may hold values from -0.375 to 0.375
- w_value: bfloat16 [4096, 4096], P('kv', 'tp'), may hold values from -0.09375 to 0.09375
- w_gate: bfloat16 [4096, 4096], P('kv', 'tp'), may hold values from -0.09375 to 0.09375
- decay_bias: float32 [2048], P('tp'), may hold values from -32 to 8
- head_gain: bfloat16 [256], replicated, may hold values from 0.099609375 to 1.8984375
- w_out: bfloat16 [4096, 4096], P('tp', 'kv'), may hold values from -0.09375 to 0.09375
- mlp_gain: bfloat16 [4096], P('tp'), may hold values from 0.099609375 to 1.8984375
- w_up: bfloat16 [4096, 16384], P('tp', 'kv'), may hold values from -0.09375 to 0.09375
- w_down: bfloat16 [16384, 4096], P('kv', 'tp'), may hold values from -0.046875 to 0.046875
Outputs:
- updated_rows: bfloat16 [512, 4096], P('kv', 'tp')
- new_state: float32 [512, 524288], P('kv', 'tp')
All inputs are finite; a program needn't handle non-finite values.
Results may differ from a plain program's by a relative error of at most 0.025.
Values may be sent and summed in bfloat16 or wider, within the bound.
A program may use at most 64 MiB of HBM per device.

v0:
```python
import jax
import jax.numpy as jnp
from jax import lax
from jax.sharding import Mesh
from jax.sharding import PartitionSpec as P

D = 4096
DK = 128
DV = 256
KV = ("kv_0", "kv_1")


epsilon = 1e-06
decay_normalizer = 16.0


def sent_to_all(shard, axis):
    copies = jnp.broadcast_to(shard, (lax.axis_size(axis), *shard.shape))
    return lax.all_to_all(copies, axis, split_axis=0, concat_axis=0, tiled=True)


def joined_along(parts, dim):
    lengths = list(parts.shape[1:])
    lengths[dim] *= parts.shape[0]
    return jnp.moveaxis(parts, 0, dim).reshape(lengths)


def gathered_copies(shard, axis, dim):
    parts = sent_to_all(shard, axis)
    return joined_along(parts, dim)


def cut_along(shard, dim, count):
    lengths = shard.shape
    parts = shard.reshape(*lengths[:dim], count, lengths[dim] // count, *lengths[dim + 1 :])
    return jnp.moveaxis(parts, dim, 0)


def sent_and_summed(shard, axis, dim):
    parts = cut_along(shard, dim, lax.axis_size(axis))
    arrived = lax.all_to_all(parts, axis, split_axis=0, concat_axis=0, tiled=True)
    return arrived.astype(jnp.float32).sum(axis=0)


def gather_axes(shard, axes, dim):
    out = shard
    for number in range(len(axes) - 1, -1, -1):
        out = lax.all_gather(out, axes[number], axis=dim, tiled=True)
    return out


def over_copies(shard, axis):
    everything = sent_to_all(shard, axis)
    return jnp.sum(everything, axis=0)


def body(
    hidden_rows,
    carried_state,
    norm_gain,
    w_query,
    w_key,
    w_decay,
    w_value,
    w_gate,
    decay_bias,
    head_gain,
    w_out,
    mlp_gain,
    w_up,
    w_down,
):
    seq_rows = hidden_rows.shape[0]
    heads_here = decay_bias.shape[0] // DK
    gathered = gathered_copies(hidden_rows, "tp", 1)
    whole_inputs = gathered.astype(jnp.float32)
    normed = (
        whole_inputs
        * lax.rsqrt(jnp.mean(whole_inputs * whole_inputs, axis=-1, keepdims=True) + epsilon)
        * norm_gain.astype(jnp.float32)
    ).astype(jnp.bfloat16)
    weights = (w_query, w_key, w_decay, w_value, w_gate)
    feature_blocks = lax.all_to_all(normed, KV, split_axis=1, concat_axis=0, tiled=True)
    joined = jnp.concatenate(weights, axis=1)
    block_rows = feature_blocks
    summed = sent_and_summed(
        jnp.dot(block_rows, joined, preferred_element_type=jnp.float32).astype(jnp.bfloat16), KV, 0
    )
    projected = []
    offset = 0
    for weight in weights:
        projected.append(summed[:, offset : offset + weight.shape[1]])
        offset = offset + weight.shape[1]
    queries, keys_new, decay_pre, values, out_gate = [
        item.astype(jnp.bfloat16) for item in projected
    ]
    log_decay = jax.nn.log_sigmoid(decay_pre.astype(jnp.float32) + decay_bias) / decay_normalizer
    log_decay = log_decay.reshape(seq_rows, heads_here, DK)
    carried = carried_state.reshape(seq_rows, heads_here, DK, DV)
    key_heads = keys_new.astype(jnp.float32).reshape(seq_rows, heads_here, DK)
    value_heads = values.astype(jnp.float32).reshape(seq_rows, heads_here, DV)
    new_state = (
        jnp.exp(log_decay)[..., None] * carried + key_heads[..., None] * value_heads[..., None, :]
    )
    query_heads = queries.astype(jnp.float32).reshape(seq_rows, heads_here, DK) * DK ** (-0.5)
    head_out = jnp.einsum("bhk,bhkv->bhv", query_heads, new_state, precision=lax.Precision.HIGHEST)
    gate_heads = out_gate.astype(jnp.float32).reshape(seq_rows, heads_here, DV)
    mixed = head_out * lax.rsqrt(jnp.mean(head_out * head_out, axis=-1, keepdims=True) + epsilon)
    mixed = (mixed * head_gain.astype(jnp.float32) * jax.nn.silu(gate_heads)).astype(jnp.bfloat16)
    mixed = mixed.reshape(seq_rows, heads_here * DV)
    partial_out = jnp.dot(
        mixed, gather_axes(w_out, KV, 1), preferred_element_type=jnp.float32
    ).astype(jnp.bfloat16)
    attn_out = sent_and_summed(
        partial_out.astype(jnp.float32).astype(jnp.bfloat16), "tp", 1
    ).astype(jnp.bfloat16)
    residual = (hidden_rows.astype(jnp.float32) + attn_out.astype(jnp.float32)).astype(jnp.bfloat16)
    resid_float = residual.astype(jnp.float32)
    total_squares = over_copies(jnp.sum(resid_float * resid_float, axis=-1), "tp")
    row_scale = lax.rsqrt(total_squares / D + epsilon)
    mlp_input = (resid_float * row_scale[:, None] * mlp_gain.astype(jnp.float32)).astype(
        jnp.bfloat16
    )
    up_partial = jnp.dot(
        gathered_copies(mlp_input, KV, 0), w_up, preferred_element_type=jnp.float32
    ).astype(jnp.bfloat16)
    up_share = sent_and_summed(up_partial.astype(jnp.float32).astype(jnp.bfloat16), "tp", 1)
    active_share = jnp.square(jax.nn.relu(up_share)).astype(jnp.bfloat16)
    activation = gathered_copies(active_share, "tp", 1)
    block_rows = activation
    mlp_total = sent_and_summed(
        jnp.dot(block_rows, w_down, preferred_element_type=jnp.float32).astype(jnp.bfloat16), KV, 0
    )
    mlp_out = mlp_total.astype(jnp.bfloat16)
    updated_rows = (resid_float + mlp_out.astype(jnp.float32)).astype(jnp.bfloat16)
    return (updated_rows, new_state.reshape(seq_rows, heads_here * DK * DV))


def solution(mesh):
    finer = Mesh(mesh.devices.reshape(8, 4, mesh.shape["tp"]), ("kv_0", "kv_1", "tp"))
    placed = (
        P(KV, "tp"),
        P(KV, "tp"),
        P(),
        P(KV, "tp"),
        P(KV, "tp"),
        P(KV, "tp"),
        P(KV, "tp"),
        P(KV, "tp"),
        P("tp"),
        P(),
        P("tp", KV),
        P("tp"),
        P("tp", KV),
        P(KV, "tp"),
    )
    return jax.shard_map(
        body, mesh=finer, in_specs=placed, out_specs=(P(KV, "tp"), P(KV, "tp")), check_vma=False
    )
```

profile of v0, /device:TPU:2, one launch (start us, length us, event | category | flops | bytes accessed | tf_op | source)
XLA Modules:
  0.0 234.3 jit_solution(10777401963919278012)
XLA Ops:
  7.3 15.8 %all_gather.6 = bf16[512,512]{1,0:T(8,128)(2,1)} all-gather(bf16[512,128]{1,0:T(8,128)(2,1)} %param.24), channel_id=1, replica_groups=mesh['kv_0'=8,'kv_1'=4,'tp'=8] {'kv_1'}, dimensions={1}, use_global_device_ids=true | all-gather | bytes 655360 | tf_op jit(solution)/shard_map/all_gather | solution.py:48
  23.1 1.4 broadcast_in_dim.8
  24.5 4.8 %all-to-all-start = ((bf16[8,16,512]{2,1,0:T(8,128)(2,1)}), bf16[8,16,512]{2,1,0:T(8,128)(2,1)S(1)}, u32[]{:S(2)}, u32[]{:S(2)}) async-start(bf16[8,16,512]{2,1,0:T(8,128)(2,1)} %broadcast_in_dim.8), calls=%async_computation | async-start | bytes 262144 | tf_op jit(solution)/shard_map/all_to_all | solution.py:19
  31.7 2.3 all-to-all-done
  35.2 11.2 %all-to-all-start.1 = ((bf16[16,32,128]{2,0,1:T(8,128)(2,1)}), bf16[16,32,128]{2,0,1:T(8,128)(2,1)S(1)}, u32[]{:S(2)}, u32[]{:S(2)}) async-start(bf16[16,32,128]{2,0,1:T(8,128)(2,1)} %copy.24), calls=%async_computation.1 | async-start | bytes 262144 | tf_op jit(solution)/shard_map/all_to_all | solution.py:83
  46.5 12.4 %all-to-all-done.1 = bf16[16,32,128]{2,0,1:T(8,128)(2,1)S(1)} async-done(((bf16[16,32,128]{2,0,1:T(8,128)(2,1)}), bf16[16,32,128]{2,0,1:T(8,128)(2,1)S(1)}, u32[]{:S(2)}, u32[]{:S(2)}) %all-to-all-start.1) | async-done | bytes 131104 | tf_op jit(solution)/shard_map/all_to_all | solution.py:83
  58.9 1.9 convolution_convert_fusion.1
  60.8 4.0 %all-to-all-start.2 = ((bf16[32,16,1792]{2,1,0:T(8,128)(2,1)}), bf16[32,16,1792]{2,1,0:T(8,128)(2,1)S(1)}, u32[]{:S(2)}, u32[]{:S(2)}) async-start(bf16[32,16,1792]{2,1,0:T(8,128)(2,1)} %bitcast.4), calls=%async_computation.2 | async-start | bytes 3670016 | tf_op jit(solution)/shard_map/all_to_all | solution.py:41
  64.8 5.5 %copy.30 = f32[2,8,256,256]{3,2,1,0:T(8,128)} copy(f32[2,8,256,256]{3,1,2,0:T(8,128)} %bitcast.60) | data formatting | bytes 8388608
  70.3 54.4 %all-to-all-done.2 = bf16[32,16,1792]{2,1,0:T(8,128)(2,1)S(1)} async-done(((bf16[32,16,1792]{2,1,0:T(8,128)(2,1)}), bf16[32,16,1792]{2,1,0:T(8,128)(2,1)S(1)}, u32[]{:S(2)}, u32[]{:S(2)}) %all-to-all-start.2) | async-done | bytes 1835040 | tf_op jit(solution)/shard_map/all_to_all | solution.py:41
  125.1 4.5 %fusion = f32[16,2,1,256]{3,2,1,0:T(1,128)S(1)} fusion(f32[16,2,128,1]{2,3,1,0:T(1,128)S(1)} %bitcast.69, f32[16,2,128,256]{3,2,1,0:T(8,128)} %bitcast.57, f32[16,2,128]{2,1,0:T(2,128)S(1)} %exp.21, f32[16,2,256]{2,1,0:T(2,128)S(1)} %reshape.111, f32[16,2,128]{2,1,0:T(2,128)S(1)} %reshape.110), kind=kOutput, calls=%fused_computation.2 | convolution fusion | flops 15728640 | bytes 4308992 | tf_op jit(solution)/shard_map/bhk,bhkv->bhv/dot_general | solution.py:106
  129.9 2.8 %convolution_convert_fusion = bf16[16,4096]{1,0:T(8,128)(2,1)S(1)} fusion(bf16[16,512]{1,0:T(8,128)(2,1)S(1)} %bitcast.70, bf16[512,4096]{1,0:T(8,128)(2,1)} %all-gather.2.cloned.1.call-done), kind=kOutput, calls=%fused_computation | convolution fusion | flops 67174400 | bytes 4341760 | tf_op jit(solution)/shard_map/dot_general | solution.py:111
  132.7 9.2 %all_to_all.57 = bf16[8,16,512]{2,1,0:T(8,128)(2,1)S(1)} all-to-all(bf16[8,16,512]{2,1,0:T(8,128)(2,1)S(1)} %bitcast.68), channel_id=1, replica_groups=mesh['kv_0'=8,'kv_1'=4,'tp'=8] {'tp'}, dimensions={0} | all-to-all | bytes 262144 | tf_op jit(solution)/shard_map/all_to_all | solution.py:41
  142.7 4.7 %all-to-all-start.4 = ((f32[8,1,16]{2,1,0:T(1,128)}), f32[8,1,16]{2,1,0:T(1,128)S(1)}, u32[]{:S(2)}, u32[]{:S(2)}) async-start(f32[8,1,16]{2,1,0:T(1,128)} %broadcast_in_dim.9), calls=%async_computation.4 | async-start | bytes 8192 | tf_op jit(solution)/shard_map/all_to_all | solution.py:19
  147.4 3.8 %all-to-all-done.4 = f32[8,1,16]{2,1,0:T(1,128)S(1)} async-done(((f32[8,1,16]{2,1,0:T(1,128)}), f32[8,1,16]{2,1,0:T(1,128)S(1)}, u32[]{:S(2)}, u32[]{:S(2)}) %all-to-all-start.4) | async-done | bytes 544 | tf_op jit(solution)/shard_map/all_to_all | solution.py:19
  151.4 22.3 %all_to_all.58 = bf16[32,16,512]{2,1,0:T(8,128)(2,1)S(1)} all-to-all(bf16[32,16,512]{2,1,0:T(8,128)(2,1)S(1)} %broadcast_in_dim.10), channel_id=1, replica_groups=mesh['kv_0'=8,'kv_1'=4,'tp'=8] {'kv_0','kv_1'}, dimensions={0} | all-to-all | bytes 1048576 | tf_op jit(solution)/shard_map/all_to_all | solution.py:19
  174.2 12.8 %all_to_all.59 = bf16[8,512,64]{1,2,0:T(8,128)(2,1)S(1)} all-to-all(bf16[8,512,64]{1,2,0:T(8,128)(2,1)S(1)} %bitcast.64), channel_id=1, replica_groups=mesh['kv_0'=8,'kv_1'=4,'tp'=8] {'tp'}, dimensions={0} | all-to-all | bytes 1048576 | tf_op jit(solution)/shard_map/all_to_all | solution.py:41
  187.9 4.9 %all-to-all-start.7 = ((bf16[8,512,64]{1,2,0:T(8,128)(2,1)}), bf16[8,512,64]{1,2,0:T(8,128)(2,1)S(1)}, u32[]{:S(2)}, u32[]{:S(2)}) async-start(bf16[8,512,64]{1,2,0:T(8,128)(2,1)} %broadcast_in_dim.11), calls=%async_computation.7 | async-start | bytes 1048576 | tf_op jit(solution)/shard_map/all_to_all | solution.py:19
  193.3 4.4 %copy.33 = f32[2,8,256,256]{3,1,2,0:T(8,128)} copy(f32[2,8,256,256]{3,2,1,0:T(8,128)S(1)} %bitcast.58) | data formatting | bytes 8388608
  198.4 4.4 %copy.32 = f32[2,8,256,256]{3,1,2,0:T(8,128)} copy(f32[2,8,256,256]{3,2,1,0:T(8,128)S(1)} %bitcast.59) | data formatting | bytes 8388608
  202.8 1.3 convolution_convert_fusion.2
  204.0 4.7 %all-to-all-start.8 = ((bf16[32,16,512]{2,1,0:T(8,128)(2,1)}), bf16[32,16,512]{2,1,0:T(8,128)(2,1)S(1)}, u32[]{:S(2)}, u32[]{:S(2)}) async-start(bf16[32,16,512]{2,1,0:T(8,128)(2,1)} %bitcast.14), calls=%async_computation.8 | async-start | bytes 1048576 | tf_op jit(solution)/shard_map/all_to_all | solution.py:41
  208.7 7.2 %multiply_add_fusion = f32[16,65536]{1,0:T(8,128)} fusion(f32[16,65536]{1,0:T(8,128)} %bitcast.61, f32[16,65536]{1,0:T(8,128)} %bitcast.62, f32[16,65536]{1,0:T(8,128)} %param.15), kind=kLoop, calls=%fused_computation.1 | loop fusion | flops 2097152 | bytes 16777216 | tf_op jit(solution)/shard_map/add | solution.py:103
  215.9 10.9 %all-to-all-done.8 = bf16[32,16,512]{2,1,0:T(8,128)(2,1)S(1)} async-done(((bf16[32,16,512]{2,1,0:T(8,128)(2,1)}), bf16[32,16,512]{2,1,0:T(8,128)(2,1)S(1)}, u32[]{:S(2)}, u32[]{:S(2)}) %all-to-all-start.8) | async-done | bytes 524320 | tf_op jit(solution)/shard_map/all_to_all | solution.py:41
  (66 shorter events, 8.5 us)
Async XLA Ops:
  7.2 166.5 %copy-start = (bf16[512,512]{1,0:T(8,128)(2,1)S(1)}, bf16[512,512]{1,0:T(8,128)(2,1)}, u32[]{:S(2)}) copy-start(bf16[512,512]{1,0:T(8,128)(2,1)} %param.26) | copy-start | bytes 1572868
  7.2 39.2 %copy-start.4 = (bf16[128,256]{1,0:T(8,128)(2,1)S(1)}, bf16[128,256]{1,0:T(8,128)(2,1)}, u32[]{:S(2)}) copy-start(bf16[128,256]{1,0:T(8,128)(2,1)} %param.19) | copy-start | bytes 196612
  7.2 39.2 %copy-start.2 = (bf16[128,512]{1,0:T(8,128)(2,1)S(1)}, bf16[128,512]{1,0:T(8,128)(2,1)}, u32[]{:S(2)}) copy-start(bf16[128,512]{1,0:T(8,128)(2,1)} %param.20) | copy-start | bytes 393220
  7.2 39.3 %copy-start.3 = (bf16[128,512]{1,0:T(8,128)(2,1)S(1)}, bf16[128,512]{1,0:T(8,128)(2,1)}, u32[]{:S(2)}) copy-start(bf16[128,512]{1,0:T(8,128)(2,1)} %param.21) | copy-start | bytes 393220
  7.2 122.6 %all-gather.2.cloned.1.call-start = ((), (), s32[]{:S(2)}) async-start(), calls=%async_computation.9 | async-start | bytes 4718592 | tf_op jit(solution)/shard_map/all_gather | solution.py:48
  24.5 9.5 %all-to-all-start = ((bf16[8,16,512]{2,1,0:T(8,128)(2,1)}), bf16[8,16,512]{2,1,0:T(8,128)(2,1)S(1)}, u32[]{:S(2)}, u32[]{:S(2)}) async-start(bf16[8,16,512]{2,1,0:T(8,128)(2,1)} %broadcast_in_dim.8), calls=%async_computation | async-start | bytes 262144 | tf_op jit(solution)/shard_map/all_to_all | solution.py:19
  35.2 23.7 %all-to-all-start.1 = ((bf16[16,32,128]{2,0,1:T(8,128)(2,1)}), bf16[16,32,128]{2,0,1:T(8,128)(2,1)S(1)}, u32[]{:S(2)}, u32[]{:S(2)}) async-start(bf16[16,32,128]{2,0,1:T(8,128)(2,1)} %copy.24), calls=%async_computation.1 | async-start | bytes 262144 | tf_op jit(solution)/shard_map/all_to_all | solution.py:83
  60.8 63.9 %all-to-all-start.2 = ((bf16[32,16,1792]{2,1,0:T(8,128)(2,1)}), bf16[32,16,1792]{2,1,0:T(8,128)(2,1)S(1)}, u32[]{:S(2)}, u32[]{:S(2)}) async-start(bf16[32,16,1792]{2,1,0:T(8,128)(2,1)} %bitcast.4), calls=%async_computation.2 | async-start | bytes 3670016 | tf_op jit(solution)/shard_map/all_to_all | solution.py:41
  64.8 5.5 %copy-start.8 = (bf16[256]{0:T(256)(128)(2,1)S(1)}, bf16[256]{0:T(256)(128)(2,1)}, u32[]{:S(2)}) copy-start(bf16[256]{0:T(256)(128)(2,1)} %param.23) | copy-start | bytes 1540
  64.8 60.2 %copy-start.5 = (f32[256]{0:T(256)S(1)}, f32[256]{0:T(256)}, u32[]{:S(2)}) copy-start(f32[256]{0:T(256)} %param.22) | copy-start | bytes 3076
  125.1 16.9 %copy-start.1 = (bf16[16,512]{1,0:T(8,128)(2,1)S(1)}, bf16[16,512]{1,0:T(8,128)(2,1)}, u32[]{:S(2)}) copy-start(bf16[16,512]{1,0:T(8,128)(2,1)} %param.14) | copy-start | bytes 49156
  125.1 22.3 %copy-start.6 = (bf16[512]{0:T(512)(128)(2,1)S(1)}, bf16[512]{0:T(512)(128)(2,1)}, u32[]{:S(2)}) copy-start(bf16[512]{0:T(512)(128)(2,1)} %param.25) | copy-start | bytes 3076
  142.7 8.5 %all-to-all-start.4 = ((f32[8,1,16]{2,1,0:T(1,128)}), f32[8,1,16]{2,1,0:T(1,128)S(1)}, u32[]{:S(2)}, u32[]{:S(2)}) async-start(f32[8,1,16]{2,1,0:T(1,128)} %broadcast_in_dim.9), calls=%async_computation.4 | async-start | bytes 8192 | tf_op jit(solution)/shard_map/all_to_all | solution.py:19
  187.9 14.9 %all-to-all-start.7 = ((bf16[8,512,64]{1,2,0:T(8,128)(2,1)}), bf16[8,512,64]{1,2,0:T(8,128)(2,1)S(1)}, u32[]{:S(2)}, u32[]{:S(2)}) async-start(bf16[8,512,64]{1,2,0:T(8,128)(2,1)} %broadcast_in_dim.11), calls=%async_computation.7 | async-start | bytes 1048576 | tf_op jit(solution)/shard_map/all_to_all | solution.py:19
  198.4 4.4 %copy-start.7 = (bf16[512,512]{1,0:T(8,128)(2,1)S(1)}, bf16[512,512]{1,0:T(8,128)(2,1)}, u32[]{:S(2)}) copy-start(bf16[512,512]{1,0:T(8,128)(2,1)} %param.27) | copy-start | bytes 1572868
  204.0 22.7 %all-to-all-start.8 = ((bf16[32,16,512]{2,1,0:T(8,128)(2,1)}), bf16[32,16,512]{2,1,0:T(8,128)(2,1)S(1)}, u32[]{:S(2)}, u32[]{:S(2)}) async-start(bf16[32,16,512]{2,1,0:T(8,128)(2,1)} %bitcast.14), calls=%async_computation.8 | async-start | bytes 1048576 | tf_op jit(solution)/shard_map/all_to_all | solution.py:41
Sparse Core Ops, SparseCore 0:
  23.2 96.3 all-gather.1
where the time goes:
time: 235 us; the launch traced here: 234 us
  waiting for transfers between devices  83.7 us (36%)
  blocking collectives  60.1 us (26%)
  starting transfers between devices  34.3 us (15%)
  local copies, waits for them, and re-layouts  20.5 us (9%)
  between operations  14.4 us (6%)
  matrix products  10.9 us (5%)
  other arithmetic  10.3 us (4%)
    all_to_all x2, waiting for transfers between devices, sent_and_summed(): lax.all_to_all(parts, axis, split_axis=0, concat_axis=0, tiled=True)  65.2 us
    all_to_all x1, blocking collectives, sent_to_all(): return lax.all_to_all(copies, axis, split_axis=0, concat_axis=0, tiled=True)  22.3 us
    all_to_all x2, blocking collectives, sent_and_summed(): lax.all_to_all(parts, axis, split_axis=0, concat_axis=0, tiled=True)  22 us
    unnamed x26, local copies, waits for them, and re-layouts  16.1 us
    all_gather x1, blocking collectives, gather_axes(): out = lax.all_gather(out, axes[number], axis=dim, tiled=True)  15.8 us
    all_to_all x3, starting transfers between devices, sent_to_all(): return lax.all_to_all(copies, axis, split_axis=0, concat_axis=0, tiled=True)  14.4 us
    all_to_all x1, waiting for transfers between devices, body(): lax.all_to_all(normed, KV, split_axis=1, concat_axis=0, tiled=True)  12.4 us
    all_to_all x1, starting transfers between devices, body(): lax.all_to_all(normed, KV, split_axis=1, concat_axis=0, tiled=True)  11.2 us
  transfers between devices with their start and end apart: 7, of which 5 were waited for; matrix products, arithmetic and copies ran while one was open for 15% of the time, Pallas kernels for 0%

commit v1 on v0

v1 whole, which is shorter than its diff:
```python
import jax
import jax.numpy as jnp
from jax import lax
from jax.experimental import pallas as pl
from jax.experimental.pallas import tpu as pltpu
from jax.sharding import Mesh
from jax.sharding import PartitionSpec as P

D = 4096
DK = 128
DV = 256
EPS = 1e-06
MESH = pl.DeviceIdType.MESH
F32 = jnp.float32
BF16 = jnp.bfloat16
KV = ("z", "y")
TP = ("x", "c")
NZ, NY, NX, NC = 8, 4, 4, 2
NEAR = (0, 1, 7, 2, 6, 3, 5, 4)
FAR = NEAR[::-1]


def place():
    return tuple(lax.axis_index(name) for name in ("z", "y", "x", "c"))


def send(src, dst, sent, arrived, device):
    pltpu.make_async_remote_copy(
        src_ref=src, dst_ref=dst, send_sem=sent, recv_sem=arrived, device_id=device, device_id_type=MESH
    ).start()


def wait(ref, sem):
    pltpu.make_async_copy(ref, ref, sem).wait()


def greet(peers):
    barrier = pltpu.get_barrier_semaphore()
    for device in peers:
        pl.semaphore_signal(barrier, inc=1, device_id=device, device_id_type=MESH)
    pl.semaphore_wait(barrier, len(peers))


def around(index, step, count):
    return lax.rem(index + step, count)


def project_kernel(
    hid, gain, wq, wk, wd, wv, wg, wo, proj, wog,
    hx, sq, xb, wb, pb, rb,
    hx_s, hx_r, sq_s, sq_r, zb_s, zb_r, yb_s, yb_r, db_r, wb_s, wb_r, wo_s, wo_r, rb_s, rb_r,
):
    z, y, x, c = place()
    kv = NY * z + y
    tp = NC * x + c
    h = hid[...].astype(F32)
    hx[x] = (h * gain[pl.ds(tp, 1), :]).astype(BF16)
    sq[tp] = jnp.broadcast_to(jnp.sum(h * h, axis=-1, keepdims=True), (16, 128))
    peers = []
    for dz in range(NZ):
        for dy in range(NY):
            if dz or dy:
                peers.append({"z": around(z, dz, NZ), "y": around(y, dy, NY)})
        if dz:
            peers.append({"z": around(z, dz, NZ), "c": 1 - c})
    for dx in range(NX):
        for dc in range(NC):
            if dx or dc:
                peers.append({"x": around(x, dx, NX), "c": around(c, dc, NC)})
    greet(peers)

    for dx in (2, 1, 3):
        send(hx.at[x], hx.at[x], hx_s, hx_r.at[x], {"x": around(x, dx, NX)})
    for dx in range(NX):
        for dc in range(NC):
            if dx or dc:
                send(sq.at[tp], sq.at[tp], sq_s, sq_r, {"x": around(x, dx, NX), "c": around(c, dc, NC)})

    def slot(origin):
        return wog.at[:, pl.ds(pl.multiple_of(origin * 128, 128), 128)]

    up, down = around(z, 1, NZ), around(z, NZ - 1, NZ)
    send(wo, slot(z), wo_s.at[0], wo_r.at[z], {"z": up})
    send(wo, slot(z), wo_s.at[1], wo_r.at[z], {"z": down})
    wog[:, pl.ds(pl.multiple_of(z * 128, 128), 128)] = wo[...]

    def pass_on(step):
        low = around(z, NZ - step + 1, NZ)
        wait(slot(low), wo_r.at[low])
        send(slot(low), slot(low), wo_s.at[2 * step - 2], wo_r.at[low], {"z": up})
        high = around(z, step - 1, NZ)
        wait(slot(high), wo_r.at[high])
        if step < 4:
            send(slot(high), slot(high), wo_s.at[2 * step - 1], wo_r.at[high], {"z": down})

    mine = pl.ds(pl.multiple_of(0, 128), 128)
    pieces = (
        (0, wv, slice(0, 512)),
        (1, wg, slice(0, 512)),
        (2, wq, slice(0, 256)),
        (2, wk, slice(256, 512)),
        (3, wd, slice(0, 256)),
    )
    for number, (home, array, columns) in enumerate(pieces):
        target = wb.at[y, :, columns]

        @pl.when(y != home)
        def _():
            send(array, target, wb_s.at[number], wb_r, {"y": home})

        @pl.when(y == home)
        def _():
            pltpu.make_async_copy(array, target, wb_r).start()

    def half(ref, number, which):
        return ref.at[number, :, pl.ds(pl.multiple_of(which * 256, 256), 256)]

    for dx in (0, 1, 3, 2):
        xs = around(x, dx, NX)
        if dx:
            wait(hx.at[xs], hx_r.at[xs])
        zt = NC * xs + c
        for dc in range(NC):
            side = around(c, dc, NC)
            src, dst = half(hx, xs, side), half(xb, kv, side)
            if dc:
                send(src, dst, zb_s.at[2 * dx + dc], zb_r.at[z], {"z": zt, "c": side})
            else:

                @pl.when(zt != z)
                def _():
                    send(src, dst, zb_s.at[2 * dx], zb_r.at[z], {"z": zt, "c": side})

                @pl.when(zt == z)
                def _():
                    pltpu.make_async_copy(src, dst, zb_r.at[z]).start()

    pass_on(2)
    for dz in NEAR:
        number = NY * around(z, dz, NZ) + y
        piece = half(xb, number, c)
        wait(piece, zb_r.at[around(z, dz, NZ)])
        for dy in (2, 1, 3):
            send(piece, piece, yb_s, yb_r.at[number], {"y": around(y, dy, NY)})
        send(piece, piece, yb_s, db_r, {"c": 1 - c})
    pass_on(3)
    for dz in NEAR:
        for dy in (1, 3, 2):
            number = NY * around(z, dz, NZ) + around(y, dy, NY)
            piece = half(xb, number, c)
            wait(piece, yb_r.at[number])
            send(piece, piece, yb_s, db_r, {"c": 1 - c})

    @pl.when(y < 3)
    def _():
        wait(wb, wb_r)

    @pl.when(y == 3)
    def _():
        wait(wb.at[:, :, slice(0, 256)], wb_r)

    wait(xb.at[:, :, slice(0, 256)], db_r)
    weights = wb[...].reshape(512, 512)

    def scatter(steps, width):
        for dz in steps:
            zt = around(z, dz, NZ)
            for dy in (2, 1, 3, 0):
                yt = around(y, dy, NY)
                src = pb.at[NY * zt + yt, :, slice(0, width)]
                dst = rb.at[y, z, :, slice(0, width)]
                if dz or dy:
                    send(src, dst, rb_s, rb_r.at[y], {"z": zt, "y": yt})
                else:
                    pltpu.make_async_copy(src, dst, rb_r.at[y]).start()

    groups = (FAR[:4], FAR[4:])
    for number, steps in enumerate(groups):
        rows = [xb[pl.ds(pl.multiple_of(NY * around(z, dz, NZ), NY), NY)].reshape(64, 512) for dz in steps]
        part = jnp.dot(jnp.concatenate(rows, axis=0), weights, preferred_element_type=F32).astype(BF16)
        for place_in, dz in enumerate(steps):
            zt = around(z, dz, NZ)
            pb[pl.ds(pl.multiple_of(NY * zt, NY), NY)] = part[64 * place_in : 64 * place_in + 64].reshape(NY, 16, 512)
        if number == 0:
            pass_on(4)

        @pl.when(y < 3)
        def _():
            scatter(steps, 512)

        @pl.when(y == 3)
        def _():
            scatter(steps, 256)

    wait(sq.at[pl.ds(0, 7)], sq_r)
    scale = lax.rsqrt(jnp.sum(sq[...], axis=0) / D + EPS)[:, 0:1]
    offset = 0
    for block, width in ((3, 256), (2, 512), (0, 512), (1, 512)):
        wait(rb.at[block, :, :, slice(0, width)], rb_r.at[block])
        total = jnp.sum(rb[block, :, :, 0:width].astype(F32), axis=0)
        proj[:, offset : offset + width] = (total * scale).astype(BF16)
        offset += width

    last = around(z, 4, NZ)
    wait(slot(last), wo_r.at[last])
    wait(hx.at[pl.ds(0, 3)], hx_s)
    wait(sq.at[pl.ds(0, 7)], sq_s)
    for number in range(7):
        wait(wo, wo_s.at[number])
    for number, (home, array, columns) in enumerate(pieces):

        @pl.when(y != home)
        def _():
            wait(array, wb_s.at[number])

    for dx in range(NX):
        wait(half(hx, 0, 0), zb_s.at[2 * dx + 1])

        @pl.when(NC * around(x, dx, NX) + c != z)
        def _():
            wait(half(hx, 0, 0), zb_s.at[2 * dx])

    wait(xb.at[pl.ds(0, 28)], yb_s)

    @pl.when(y < 3)
    def _():
        wait(pb.at[pl.ds(0, 31)], rb_s)

    @pl.when(y == 3)
    def _():
        wait(pb.at[pl.ds(0, 31), :, slice(0, 256)], rb_s)


def project(hid, gain, wq, wk, wd, wv, wg, wo):
    dma = pltpu.SemaphoreType.DMA
    vmem = pl.BlockSpec(memory_space=pltpu.VMEM)
    return pl.pallas_call(
        project_kernel,
        out_shape=(jax.ShapeDtypeStruct((16, 1792), BF16), jax.ShapeDtypeStruct((512, 1024), BF16)),
        in_specs=[vmem] * 8,
        out_specs=(vmem, vmem),
        scratch_shapes=[
            pltpu.VMEM((NX, 16, 512), BF16),
            pltpu.VMEM((8, 16, 128), F32),
            pltpu.VMEM((32, 16, 512), BF16),
            pltpu.VMEM((NY, 128, 512), BF16),
            pltpu.VMEM((32, 16, 512), BF16),
            pltpu.VMEM((NY, NZ, 16, 512), BF16),
            dma, dma((NX,)), dma, dma, dma((8,)), dma((NZ,)), dma, dma((32,)), dma,
            dma((5,)), dma, dma((7,)), dma((NZ,)), dma, dma((NY,)),
        ],
        compiler_params=pltpu.CompilerParams(collective_id=0, has_side_effects=True),
        name="project",
    )(hid, gain, wq, wk, wd, wv, wg, wo)


STEPS = 16
WIDE = 65536 // STEPS
KEYS = WIDE // DV


def state_kernel(proj, bias, head_gain, state, new_state, mixed, decay, acc):
    step = pl.program_id(0)
    per_head = DK // KEYS

    @pl.when(step == 0)
    def _():
        pre = proj[:, 0:256].astype(F32) + bias[...]
        soft = jnp.minimum(pre, 0.0) - jnp.log1p(jnp.exp(-jnp.abs(pre)))
        decay[...] = jnp.exp(soft / 16.0)
        acc[...] = jnp.zeros_like(acc)

    head = step // per_head
    back = 256 - step * KEYS
    shift = lax.rem(back, 256)
    rates = pltpu.roll(decay[...], shift, axis=1)
    queries = pltpu.roll(proj[:, 256:512].astype(F32) * DK ** (-0.5), shift, axis=1)
    keys = pltpu.roll(proj[:, 512:768].astype(F32), shift, axis=1)
    columns = pl.ds(pl.multiple_of(head * DV, DV), DV)
    values = proj[:, pl.ds(pl.multiple_of(768 + head * DV, DV), DV)].astype(F32)
    total = acc[:, columns]
    for key in range(KEYS):
        where = slice(key * DV, key * DV + DV)
        fresh = rates[:, key : key + 1] * state[:, where] + keys[:, key : key + 1] * values
        new_state[:, where] = fresh
        total = total + queries[:, key : key + 1] * fresh
    acc[:, columns] = total

    @pl.when(step == STEPS - 1)
    def _():
        for number in range(2):
            part = slice(number * DV, number * DV + DV)
            out = acc[:, part]
            gate = proj[:, 1280 + number * DV : 1280 + number * DV + DV].astype(F32)
            normal = out * lax.rsqrt(jnp.mean(out * out, axis=-1, keepdims=True) + EPS)
            silu = gate / (1.0 + jnp.exp(-gate))
            mixed[:, part] = (normal * head_gain[...].astype(F32) * silu).astype(BF16)


def update_state(proj, bias, head_gain, state):
    fixed = lambda *shape: pl.BlockSpec(shape, lambda i: (0,) * len(shape))
    return pl.pallas_call(
        state_kernel,
        grid=(STEPS,),
        out_shape=(jax.ShapeDtypeStruct((16, 65536), F32), jax.ShapeDtypeStruct((16, 512), BF16)),
        in_specs=[fixed(16, 1792), fixed(1, 256), fixed(1, 256), pl.BlockSpec((16, WIDE), lambda i: (0, i))],
        out_specs=(pl.BlockSpec((16, WIDE), lambda i: (0, i)), fixed(16, 512)),
        scratch_shapes=[pltpu.VMEM((16, 256), F32), pltpu.VMEM((16, 512), F32)],
        compiler_params=pltpu.CompilerParams(dimension_semantics=("arbitrary",)),
        name="update_state",
    )(proj, bias, head_gain, state)


def feed_kernel(
    mixed, wog, hid, gain, wu_hbm, wd_hbm, out,
    wu, wd, mb, hp, op, r2, rp, res, sq, upb, dd, us, ur, act, dp, dy_b, zs, zr,
    w_sem, mb_s, mb_r, hp_s, hp_r, op_s, op_r, rz_s, rz_r, ry_s, ry_r, sq_s, sq_r,
    dd_s, dd_r, us_s, us_r, ac_s, ac_r, ad_r, dy_s, dy_r, zr_s, zr_r,
):
    z, y, x, c = place()
    tp = NC * x + c
    pltpu.make_async_copy(wu_hbm, wu, w_sem.at[0]).start()
    pltpu.make_async_copy(wd_hbm, wd, w_sem.at[1]).start()
    mb[y] = mixed[...]
    tps = [
        {"x": around(x, dx, NX), "c": around(c, dc, NC)} for dx in (2, 1, 3, 0) for dc in range(NC) if dx or dc
    ]
    ys = [{"y": around(y, dy, NY)} for dy in (2, 1, 3)]
    zs_far = [{"z": around(z, dz, NZ)} for dz in FAR[:7]]
    greet(tps + ys + zs_far)

    for device in ys:
        send(mb.at[y], mb.at[y], mb_s, mb_r, device)
    for dy in (2, 1, 3):
        yt = around(y, dy, NY)
        columns = pl.ds(pl.multiple_of(yt * 128, 128), 128)
        send(hid.at[:, columns], hp.at[y], hp_s, hp_r, {"y": yt})
    here = pl.ds(pl.multiple_of(y * 128, 128), 128)
    hp[y] = hid[:, here]
    wait(mb.at[pl.ds(0, 3)], mb_r)
    part = jnp.dot(mb[...].reshape(64, 512), wog[...], preferred_element_type=F32).astype(BF16)
    for t in range(8):
        op[t] = part[:, t * 128 : t * 128 + 128]
    r2[tp] = op[tp]
    for device in tps:
        t = NC * device["x"] + device["c"]
        send(op.at[t], r2.at[tp], op_s, op_r, device)
    wait(hp.at[pl.ds(0, 3)], hp_r)
    wait(r2.at[pl.ds(0, 7)], op_r)
    attn = jnp.sum(r2[...].astype(F32), axis=0).astype(BF16).astype(F32)
    rp[...] = (hp[...].reshape(64, 128).astype(F32) + attn).astype(BF16)
    res[z, :, here] = rp[...]
    for device in zs_far:
        send(rp, res.at[z, :, here], rz_s, rz_r.at[z], device)
    for dz in NEAR:
        zt = around(z, dz, NZ)
        piece = res.at[zt, :, here]
        if dz:
            wait(piece, rz_r.at[zt])
        for device in ys:
            send(piece, piece, ry_s, ry_r.at[NY * zt + y], device)

    def arrived(zt):
        for dy in (1, 3, 2):
            yt = around(y, dy, NY)
            piece = res.at[zt, :, pl.ds(pl.multiple_of(yt * 128, 128), 128)]
            wait(piece, ry_r.at[NY * zt + yt])

    rows = pl.ds(pl.multiple_of(y * 16, 16), 16)
    pltpu.make_async_copy(wu_hbm, wu, w_sem.at[0]).wait()
    pair_near = (0, 1, 3, 2)
    first = z // 2
    for dp_ in pair_near:
        i = around(first, dp_, 4)
        arrived(2 * i)
        arrived(2 * i + 1)
        both = res[pl.ds(pl.multiple_of(2 * i, 2), 2)].reshape(128, 512).astype(F32)
        fed = (both * gain[...].astype(F32)).astype(BF16)
        part = jnp.dot(fed, wu[...], preferred_element_type=F32).astype(BF16)
        upb[pl.ds(pl.multiple_of(2 * i, 2), 2)] = part.reshape(2, 64, 512)
        send(upb.at[2 * i + 1 - c], dd.at[i], dd_s, dd_r.at[i], {"c": 1 - c})
        if dp_ == 0:
            own = res[z, rows, :].astype(F32)
            sq[tp] = jnp.broadcast_to(jnp.sum(own * own, axis=-1, keepdims=True), (16, 128))
    for device in tps:
        send(sq.at[tp], sq.at[tp], sq_s, sq_r, device)
    for dp_ in pair_near:
        i = around(first, dp_, 4)
        wait(dd.at[i], dd_r.at[i])
        us[i] = (upb[2 * i + c].astype(F32) + dd[i].astype(F32)).astype(BF16)

        @pl.when(i != x)
        def _():
            send(us.at[i], ur.at[x], us_s, us_r.at[x], {"x": i})

    total = us[x].astype(F32)
    for dx in (1, 3, 2):
        xs = around(x, dx, NX)
        wait(ur.at[xs], us_r.at[xs])
        total = total + ur[xs].astype(F32)
    act[tp] = jnp.square(jnp.maximum(total, 0.0)).astype(BF16)
    for dx in (2, 1, 3):
        send(act.at[tp], act.at[tp], ac_s, ac_r.at[x], {"x": around(x, dx, NX)})
    send(act.at[tp], act.at[tp], ac_s, ad_r.at[x], {"c": 1 - c})
    pltpu.make_async_copy(wd_hbm, wd, w_sem.at[1]).wait()
    for dx in (0, 1, 3, 2):
        xs = around(x, dx, NX)
        if dx:
            piece = act.at[NC * xs + c]
            wait(piece, ac_r.at[xs])
            send(piece, piece, ac_s, ad_r.at[xs], {"c": 1 - c})
    for dx in (0, 1, 3, 2):
        xs = around(x, dx, NX)
        wait(act.at[NC * xs + 1 - c], ad_r.at[xs])
        both = act[pl.ds(pl.multiple_of(2 * xs, 2), 2)].reshape(128, 512)
        part = jnp.dot(both, wd[...], preferred_element_type=F32).astype(BF16)
        dp[pl.ds(pl.multiple_of(2 * xs, 2), 2)] = part.reshape(2, NY, 16, 512)
        for device in ys:
            send(
                dp.at[pl.ds(pl.multiple_of(2 * xs, 2), 2), device["y"]],
                dy_b.at[y, pl.ds(pl.multiple_of(2 * xs, 2), 2)],
                dy_s,
                dy_r.at[xs],
                device,
            )
    for dx in (0, 1, 3, 2):
        xs = around(x, dx, NX)
        two = pl.ds(pl.multiple_of(2 * xs, 2), 2)
        wait(dy_b.at[pl.ds(0, 3), two], dy_r.at[xs])
        total = dp[two, y].astype(F32)
        for dy in (1, 2, 3):
            total = total + dy_b[around(y, dy, NY), two].astype(F32)
        zs[two] = total.astype(BF16)
        for k in range(2):
            j = 2 * xs + k

            @pl.when(j != z)
            def _():
                send(zs.at[j], zr.at[z], zr_s, zr_r, {"z": j})

    zr[z] = zs[z]
    wait(sq.at[pl.ds(0, 7)], sq_r)
    wait(zr.at[pl.ds(0, 7)], zr_r)
    mean = jnp.sum(sq[...], axis=0)[:, 0:1] / D
    squared = 1.0 / (mean + EPS)
    mlp = (jnp.sum(zr[...].astype(F32), axis=0) * squared).astype(BF16).astype(F32)
    out[...] = (res[z, rows, :].astype(F32) + mlp).astype(BF16)

    wait(mb.at[pl.ds(0, 3)], mb_s)
    wait(hp.at[pl.ds(0, 3)], hp_s)
    wait(r2.at[pl.ds(0, 7)], op_s)
    wait(op.at[pl.ds(0, 7)], rz_s)
    wait(res.at[:, :, slice(0, 384)], ry_s)
    wait(sq.at[pl.ds(0, 7)], sq_s)
    wait(dd, dd_s)
    wait(us.at[pl.ds(0, 3)], us_s)
    wait(act.at[pl.ds(0, 7)], ac_s)
    wait(dy_b.at[pl.ds(0, 3)], dy_s)
    wait(zr.at[pl.ds(0, 7)], zr_s)


def feed(mixed, wog, hid, gain, w_up, w_down):
    dma = pltpu.SemaphoreType.DMA
    vmem = pl.BlockSpec(memory_space=pltpu.VMEM)
    anywhere = pl.BlockSpec(memory_space=pl.ANY)
    return pl.pallas_call(
        feed_kernel,
        out_shape=jax.ShapeDtypeStruct((16, 512), BF16),
        in_specs=[vmem] * 4 + [anywhere] * 2,
        out_specs=vmem,
        scratch_shapes=[
            pltpu.VMEM((512, 512), BF16),
            pltpu.VMEM((512, 512), BF16),
            pltpu.VMEM((NY, 16, 512), BF16),
            pltpu.VMEM((NY, 16, 128), BF16),
            pltpu.VMEM((8, 64, 128), BF16),
            pltpu.VMEM((8, 64, 128), BF16),
            pltpu.VMEM((64, 128), BF16),
            pltpu.VMEM((NZ, 64, 512), BF16),
            pltpu.VMEM((8, 16, 128), F32),
            pltpu.VMEM((8, 64, 512), BF16),
            pltpu.VMEM((4, 64, 512), BF16),
            pltpu.VMEM((4, 64, 512), BF16),
            pltpu.VMEM((4, 64, 512), BF16),
            pltpu.VMEM((8, 64, 512), BF16),
            pltpu.VMEM((8, NY, 16, 512), BF16),
            pltpu.VMEM((NY, 8, 16, 512), BF16),
            pltpu.VMEM((8, 16, 512), BF16),
            pltpu.VMEM((NZ, 16, 512), BF16),
            dma((2,)), dma, dma, dma, dma, dma, dma, dma, dma((NZ,)), dma, dma((32,)), dma, dma,
            dma, dma((4,)), dma, dma((4,)), dma, dma((4,)), dma((4,)), dma, dma((4,)), dma, dma,
        ],
        compiler_params=pltpu.CompilerParams(collective_id=1, has_side_effects=True),
        name="feed",
    )(mixed, wog, hid, gain, w_up, w_down)


def body(
    hidden_rows, carried_state, norm_gain, w_query, w_key, w_decay, w_value, w_gate,
    decay_bias, head_gain, w_out, mlp_gain, w_up, w_down,
):
    gains = norm_gain.astype(F32).reshape(8, 512)
    proj, wog = project(hidden_rows, gains, w_query, w_key, w_decay, w_value, w_gate, w_out)
    new_state, mixed = update_state(proj, decay_bias.reshape(1, 256), head_gain.reshape(1, 256), carried_state)
    updated = feed(mixed, wog, hidden_rows, mlp_gain.reshape(1, 512), w_up, w_down)
    return updated, new_state


def solution(mesh):
    finer = Mesh(mesh.devices.reshape(NZ, NY, NX, NC), ("z", "y", "x", "c"))
    placed = (
        P(KV, TP), P(KV, TP), P(), P(KV, TP), P(KV, TP), P(KV, TP), P(KV, TP), P(KV, TP),
        P(TP), P(), P(TP, KV), P(TP), P(TP, KV), P(KV, TP),
    )
    return jax.shard_map(
        body, mesh=finer, in_specs=placed, out_specs=(P(KV, TP), P(KV, TP)), check_vma=False
    )
```

time: 235 us -> 110 us (0.47)
  Pallas kernels: 0 us -> 104 us
  waiting for transfers between devices: 83.7 us -> 0 us
  blocking collectives: 60.1 us -> 0 us
  starting transfers between devices: 34.3 us -> 0 us
  local copies, waits for them, and re-layouts: 20.5 us -> 4.48 us
  between operations: 14.4 us -> 0.66 us
  matrix products: 10.9 us -> 0 us
  other arithmetic: 10.3 us -> 0 us
    pallas_call x0 -> x3, Pallas kernels: none -> 104 us  [the longest x1 49.5 us: feed(): pl.pallas_call(feed_kernel, out_shape=jax.ShapeDtypeStruct((16, 512), BF1...]
    all_to_all x6 -> x0, waiting for transfers between devices: 83.7 us -> none  [the longest x2 65.2 us: sent_and_summed(): lax.all_to_all(parts, axis, split_axis=0, concat_axis=0, tiled=True)]
    all_to_all x3 -> x0, blocking collectives: 44.3 us -> none  [the longest x1 22.3 us: sent_to_all(): return lax.all_to_all(copies, axis, split_axis=0, concat_axis=0, tiled=True)]
    all_to_all x6 -> x0, starting transfers between devices: 34.2 us -> none  [the longest x3 14.4 us: sent_to_all(): return lax.all_to_all(copies, axis, split_axis=0, concat_axis=0, tiled=True)]
    all_gather x1 -> x0, blocking collectives: 15.8 us -> none  [gather_axes(): out = lax.all_gather(out, axes[number], axis=dim, tiled=True)]
    unnamed x26 -> x3, local copies, waits for them, and re-layouts: 16.1 us -> 1.33 us
    dot_general x5 -> x0, matrix products: 10.9 us -> none  [the longest x1 4.46 us: body(): jnp.einsum('bhk,bhkv->bhv', query_heads, new_state, precision=lax.Precisi...]
    add x1 -> x0, other arithmetic: 7.22 us -> none  [body(): jnp.exp(log_decay)[..., None] * carried]
  transfers between devices with their start and end apart: 7 -> 0, of which waited for: 5 -> 0; matrix products, arithmetic and copies ran while one was open for 15% -> 0% of each run, Pallas kernels for 0% -> 0%
where the time goes in v1:
time: 110 us; the launch traced here: 109 us
  Pallas kernels  104 us (95%)
  local copies, waits for them, and re-layouts  4.48 us (4%)
    pallas_call x1, Pallas kernels, feed(): pl.pallas_call(feed_kernel, out_shape=jax.ShapeDtypeStruct((16, 512), BF1...  49.5 us
    pallas_call x1, Pallas kernels, project(): pl.pallas_call(project_kernel, out_shape=(jax.ShapeDtypeStruct((16, 1792)...  42.8 us
    pallas_call x1, Pallas kernels, update_state(): pl.pallas_call(state_kernel, grid=(STEPS,), out_shape=(jax.ShapeDtypeStru...  12 us

profile of v1, /device:TPU:2, one launch (start us, length us, event | category | flops | bytes accessed | tf_op | source)
XLA Modules:
  0.0 109.4 jit_solution(18351173747927575434)
XLA Ops:
  0.6 0.0 copy-start
  0.6 1.3 %reshape.24.gain = f32[8,512]{1,0:T(8,128)} reshape(bf16[4096]{0:T(1024)(128)(2,1)} %param.16) | data formatting | bytes 24576 | tf_op jit(solution)/shard_map/reshape | solution.py:502
  2.0 42.8 %project.1 = (bf16[16,1792]{1,0:T(8,128)(2,1)}, bf16[512,1024]{1,0:T(8,128)(2,1)}) custom-call(bf16[16,512]{1,0:T(8,128)(2,1)} %hid.3, f32[8,512]{1,0:T(8,128)} %reshape.24.gain, bf16[128,256]{1,0:T(8,128)(2,1)} %wq.1, bf16[128,256]{1,0:T(8,128)(2,1)} %wk.1, bf16[128,256]{1,0:T(8,128)(2,1)} %wd.1, bf16[128,512]{1,0:T(8,128)(2,1)} %wv.1, ...), custom_call_target="tpu_custom_call" | custom-call | tf_op jit(solution)/shard_map/project/pallas_call | solution.py:237
  44.7 1.2 %reshape.21.head_gain = bf16[1,256]{1,0:T(2,128)(2,1)} reshape(bf16[256]{0:T(256)(128)(2,1)} %param.23) | data formatting | bytes 1024 | tf_op jit(solution)/shard_map/reshape | solution.py:504
  46.0 12.0 %update_state.1 = (f32[16,65536]{1,0:T(8,128)}, bf16[16,512]{1,0:T(8,128)(2,1)}) custom-call(bf16[16,1792]{1,0:T(8,128)(2,1)} %get-tuple-element.6.proj, f32[1,256]{1,0:T(1,128)} %bitcast.1, bf16[1,256]{1,0:T(2,128)(2,1)} %reshape.21.head_gain, f32[16,65536]{1,0:T(8,128)} %state.1), custom_call_target="tpu_custom_call" | custom-call | tf_op jit(solution)/shard_map/update_state/pallas_call | solution.py:302
  58.0 0.0 copy-done
  58.0 0.6 reshape.22.gain
  58.6 49.5 %feed.1 = bf16[16,512]{1,0:T(8,128)(2,1)} custom-call(bf16[16,512]{1,0:T(8,128)(2,1)} %get-tuple-element.7.mixed, bf16[512,1024]{1,0:T(8,128)(2,1)} %get-tuple-element.8.wog, bf16[16,512]{1,0:T(8,128)(2,1)} %hid.3, bf16[1,512]{1,0:T(2,128)(2,1)} %reshape.22.gain, bf16[512,512]{1,0:T(8,128)(2,1)} %wu_hbm.1, bf16[512,512]{1,0:T(8,128)(2,1)} %wd_hbm.1), custom_call_target="tpu_custom_call" | custom-call | tf_op jit(solution)/shard_map/feed/pallas_call | solution.py:466
  108.1 1.3 %copy.17 = bf16[16,512]{1,0:T(8,128)(2,1)} copy(bf16[16,512]{1,0:T(8,128)(2,1)} %feed.1) | data formatting | bytes 32768
Async XLA Ops:
  0.6 57.4 %copy-start = (bf16[512]{0:T(512)(128)(2,1)S(1)}, bf16[512]{0:T(512)(128)(2,1)}, u32[]{:S(2)}) copy-start(bf16[512]{0:T(512)(128)(2,1)} %param.25) | copy-start | bytes 3076

commit v2 on v0

v2 whole, which is shorter than its diff:
```python
import jax
import jax.numpy as jnp
from jax import lax
from jax.experimental import pallas as pl
from jax.experimental.pallas import tpu as pltpu
from jax.sharding import Mesh
from jax.sharding import PartitionSpec as P

D = 4096
DK = 128
DV = 256
EPS = 1e-06
MESH = pl.DeviceIdType.MESH
F32 = jnp.float32
BF16 = jnp.bfloat16
KV = ("z", "y")
TP = ("x", "c")
NZ, NY, NX, NC = 8, 4, 4, 2
GROUPS = ((0, 1), (7, 2), (6, 3), (5, 4))
PAIRS = (0, 1, 3, 2)
KEYS = 32


def place():
    return tuple(lax.axis_index(name) for name in ("z", "y", "x", "c"))


def send(src, dst, sent, arrived, device):
    pltpu.make_async_remote_copy(
        src_ref=src, dst_ref=dst, send_sem=sent, recv_sem=arrived, device_id=device, device_id_type=MESH
    ).start()


def wait(ref, sem):
    pltpu.make_async_copy(ref, ref, sem).wait()


def greet(peers):
    barrier = pltpu.get_barrier_semaphore()
    for device in peers:
        pl.semaphore_signal(barrier, inc=1, device_id=device, device_id_type=MESH)
    pl.semaphore_wait(barrier, len(peers))


def around(index, step, count):
    return lax.rem(index + step, count)


def layer_kernel(
    hid_hbm, norm_gain_hbm, bias_hbm, head_gain_hbm, mlp_gain_hbm,
    wq, wk, wd, wv, wg, wo, wu_hbm, wdn_hbm, state_hbm,
    out, new_state, hid, norm_gain, bias, head_gain, mlp_gain,
    hx, sq, xb, wb, pb, rb, proj, wog, state, acc, decay,
    wu, wdn, mb, hp, op, r2, res, sq2, upb, dd, us, ur, act, dp, dyb, zs, zr,
    in_sem, hx_s, hx_r, sq_s, sq_r, zb_s, zb_r, yb_s, yb_r, db_r, wb_s, wb_r, wo_s, wo_r, rb_s, rb_r,
    mb_s, mb_r, hp_s, hp_r, op_s, op_r, rz_s, rz_r, ry_s, ry_r, sq2_s, sq2_r,
    dd_s, dd_r, us_s, us_r, ac_s, ac_r, ad_r, dy_s, dy_r, zr_s, zr_r,
):
    z, y, x, c = place()
    kv = NY * z + y
    tp = NC * x + c
    small = (
        (hid_hbm, hid), (norm_gain_hbm, norm_gain), (bias_hbm, bias), (head_gain_hbm, head_gain), (mlp_gain_hbm, mlp_gain),
    )
    for number, (src, dst) in enumerate(small):
        pltpu.make_async_copy(src, dst, in_sem.at[4 + number]).start()
    pltpu.make_async_copy(state_hbm, state, in_sem.at[0]).start()
    pltpu.make_async_copy(wu_hbm, wu, in_sem.at[1]).start()
    pltpu.make_async_copy(wdn_hbm, wdn, in_sem.at[2]).start()
    for number, (src, dst) in enumerate(small):
        pltpu.make_async_copy(src, dst, in_sem.at[4 + number]).wait()
    h = hid[...].astype(F32)
    gain = norm_gain[pl.ds(pl.multiple_of(tp * 512, 512), 512)].astype(F32).reshape(1, 512)
    hx[x] = (h * gain).astype(BF16)
    sq[tp] = jnp.broadcast_to(jnp.sum(h * h, axis=-1, keepdims=True), (16, 128))
    tps = [
        {"x": around(x, dx, NX), "c": around(c, dc, NC)} for dx in (2, 1, 3, 0) for dc in range(NC) if dx or dc
    ]
    ys = [{"y": around(y, dy, NY)} for dy in (2, 1, 3)]
    zfar = [{"z": around(z, dz, NZ)} for dz in (4, 3, 5, 2, 6, 1, 7)]
    greet(tps + zfar + [{"z": device["z"], "c": 1 - c} for device in zfar] + ys)

    def lanes(index, width):
        return pl.ds(pl.multiple_of(index * width, width), width)

    def slot(origin):
        return wog.at[:, lanes(origin, 128)]

    for dx in (2, 1, 3):
        send(hx.at[x], hx.at[x], hx_s, hx_r.at[x], {"x": around(x, dx, NX)})
    for device in tps:
        send(sq.at[tp], sq.at[tp], sq_s, sq_r, device)
    up, down = around(z, 1, NZ), around(z, NZ - 1, NZ)
    send(wo, slot(z), wo_s.at[0], wo_r.at[z], {"z": up})
    send(wo, slot(z), wo_s.at[1], wo_r.at[z], {"z": down})
    pltpu.make_async_copy(wo, slot(z), in_sem.at[3]).start()
    pieces = (
        (0, wv, slice(0, 512)),
        (1, wg, slice(0, 512)),
        (2, wq, slice(0, 256)),
        (2, wk, slice(256, 512)),
        (3, wd, slice(0, 256)),
    )
    for number, (home, array, columns) in enumerate(pieces):
        target = wb.at[y, :, columns]

        @pl.when(y != home)
        def _():
            send(array, target, wb_s.at[number], wb_r, {"y": home})

        @pl.when(y == home)
        def _():
            pltpu.make_async_copy(array, target, wb_r).start()

    for dy in (2, 1, 3):
        yt = around(y, dy, NY)
        send(hid.at[:, lanes(yt, 128)], hp.at[y], hp_s, hp_r, {"y": yt})
    hp[y] = hid[:, lanes(y, 128)]

    def pass_on(step):
        low = around(z, NZ - step + 1, NZ)
        wait(slot(low), wo_r.at[low])
        send(slot(low), slot(low), wo_s.at[2 * step - 2], wo_r.at[low], {"z": up})
        high = around(z, step - 1, NZ)
        wait(slot(high), wo_r.at[high])
        if step < 4:
            send(slot(high), slot(high), wo_s.at[2 * step - 1], wo_r.at[high], {"z": down})

    def half(ref, number, which):
        return ref.at[number, :, lanes(which, 256)]

    for dx in (0, 1, 3, 2):
        xs = around(x, dx, NX)
        if dx:
            wait(hx.at[xs], hx_r.at[xs])
        zt = NC * xs + c
        for dc in range(NC):
            side = around(c, dc, NC)
            src, dst = half(hx, xs, side), half(xb, kv, side)
            if dc:
                send(src, dst, zb_s.at[2 * dx + dc], zb_r.at[z], {"z": zt, "c": side})
            else:

                @pl.when(zt != z)
                def _():
                    send(src, dst, zb_s.at[2 * dx], zb_r.at[z], {"z": zt, "c": side})

                @pl.when(zt == z)
                def _():
                    pltpu.make_async_copy(src, dst, zb_r.at[z]).start()

    def spread_y(group):
        for dz in group:
            zt = around(z, dz, NZ)
            number = NY * zt + y
            piece = half(xb, number, c)
            wait(piece, zb_r.at[zt])
            for device in ys:
                send(piece, piece, yb_s, yb_r.at[number], device)
            send(piece, piece, yb_s, db_r.at[zt], {"c": 1 - c})

    def spread_c(group):
        for dz in group:
            zt = around(z, dz, NZ)
            for dy in (1, 3, 2):
                number = NY * zt + around(y, dy, NY)
                piece = half(xb, number, c)
                wait(piece, yb_r.at[number])
                send(piece, piece, yb_s, db_r.at[zt], {"c": 1 - c})

    def scatter(steps, width):
        for dz in steps:
            zt = around(z, dz, NZ)
            for dy in (2, 1, 3, 0):
                yt = around(y, dy, NY)
                src = pb.at[NY * zt + yt, :, slice(0, width)]
                dst = rb.at[y, z, :, slice(0, width)]
                if dz or dy:
                    send(src, dst, rb_s, rb_r.at[y], {"z": zt, "y": yt})
                else:
                    pltpu.make_async_copy(src, dst, rb_r.at[y]).start()

    def multiply(group):
        for dz in group:
            zt = around(z, dz, NZ)
            wait(xb.at[pl.ds(pl.multiple_of(NY * zt, NY), NY), :, slice(0, 256)], db_r.at[zt])
        rows = [xb[pl.ds(pl.multiple_of(NY * around(z, dz, NZ), NY), NY)].reshape(64, 512) for dz in group]
        weights = wb[...].reshape(512, 512)
        part = jnp.dot(jnp.concatenate(rows, axis=0), weights, preferred_element_type=F32).astype(BF16)
        for number, dz in enumerate(group):
            zt = around(z, dz, NZ)
            pb[pl.ds(pl.multiple_of(NY * zt, NY), NY)] = part[64 * number : 64 * number + 64].reshape(NY, 16, 512)

        @pl.when(y < 3)
        def _():
            scatter(group, 512)

        @pl.when(y == 3)
        def _():
            scatter(group, 256)

    for group in GROUPS:
        spread_y(group)
    spread_c(GROUPS[0])
    spread_c(GROUPS[1])
    pass_on(2)

    @pl.when(y < 3)
    def _():
        wait(wb, wb_r)

    @pl.when(y == 3)
    def _():
        wait(wb.at[:, :, slice(0, 256)], wb_r)

    multiply(GROUPS[0])
    spread_c(GROUPS[2])
    multiply(GROUPS[1])
    spread_c(GROUPS[3])
    multiply(GROUPS[2])
    multiply(GROUPS[3])
    pass_on(3)

    wait(sq.at[pl.ds(0, 7)], sq_r)
    scale = lax.rsqrt(jnp.sum(sq[...], axis=0) / D + EPS)[:, 0:1]

    def summed(block, width, offset):
        wait(rb.at[block, :, :, slice(0, width)], rb_r.at[block])
        total = jnp.sum(rb[block, :, :, 0:width].astype(F32), axis=0)
        proj[:, offset : offset + width] = (total * scale).astype(BF16).astype(F32)

    summed(3, 256, 0)
    summed(2, 512, 256)
    summed(0, 512, 768)
    summed(1, 512, 1280)
    pre = proj[:, 0:256] + bias[...].reshape(1, 256)
    soft = jnp.minimum(pre, 0.0) - jnp.log1p(jnp.exp(-jnp.abs(pre)))
    decay[...] = jnp.exp(soft / 16.0)
    acc[...] = jnp.zeros_like(acc)
    pltpu.make_async_copy(state_hbm, state, in_sem.at[0]).wait()

    @pl.loop(0, 256 // KEYS)
    def _(step):
        shift = lax.rem(256 - step * KEYS, 256)
        rates = pltpu.roll(decay[...], shift, axis=1)
        queries = pltpu.roll(proj[:, 256:512] * DK ** (-0.5), shift, axis=1)
        keys = pltpu.roll(proj[:, 512:768], shift, axis=1)
        head = step // (DK // KEYS)
        columns = lanes(head, DV)
        values = proj[:, pl.ds(pl.multiple_of(768 + head * DV, DV), DV)]
        total = acc[:, columns]
        for key in range(KEYS):
            where = pl.ds(pl.multiple_of((step * KEYS + key) * DV, DV), DV)
            fresh = rates[:, key : key + 1] * state[:, where] + keys[:, key : key + 1] * values
            new_state[:, where] = fresh
            total = total + queries[:, key : key + 1] * fresh
        acc[:, columns] = total

    for number in range(2):
        part = slice(number * DV, number * DV + DV)
        value = acc[:, part]
        gate = proj[:, 1280 + number * DV : 1280 + number * DV + DV]
        normal = value * lax.rsqrt(jnp.mean(value * value, axis=-1, keepdims=True) + EPS)
        silu = gate / (1.0 + jnp.exp(-gate))
        mb[y, :, part] = (normal * head_gain[...].astype(F32).reshape(1, DV) * silu).astype(BF16)
    for device in ys:
        send(mb.at[y], mb.at[y], mb_s, mb_r, device)
    pass_on(4)
    here = lanes(y, 128)
    last = around(z, 4, NZ)
    wait(slot(last), wo_r.at[last])
    pltpu.make_async_copy(wo, slot(z), in_sem.at[3]).wait()
    wait(mb.at[pl.ds(0, 3)], mb_r)
    part = jnp.dot(mb[...].reshape(64, 512), wog[...], preferred_element_type=F32).astype(BF16)
    for t in range(8):
        op[t] = part[:, t * 128 : t * 128 + 128]
    r2[tp] = op[tp]
    for device in tps:
        t = NC * device["x"] + device["c"]
        send(op.at[t], r2.at[tp], op_s, op_r, device)
    wait(hp.at[pl.ds(0, 3)], hp_r)
    wait(r2.at[pl.ds(0, 7)], op_r)
    attn = jnp.sum(r2[...].astype(F32), axis=0).astype(BF16).astype(F32)
    res[z, :, here] = (hp[...].reshape(64, 128).astype(F32) + attn).astype(BF16)
    mine = res.at[z, :, here]
    for device in zfar:
        send(mine, mine, rz_s, rz_r.at[z], device)
    for device in ys:
        send(mine, mine, ry_s, ry_r.at[kv], device)

    rows = pl.ds(pl.multiple_of(y * 16, 16), 16)
    first = z // 2

    def two(pair):
        return pl.ds(pl.multiple_of(2 * pair, 2), 2)

    def relay(pair):
        for k in range(2):
            zt = 2 * pair + k
            piece = res.at[zt, :, here]

            @pl.when(zt != z)
            def _():
                wait(piece, rz_r.at[zt])
                for device in ys:
                    send(piece, piece, ry_s, ry_r.at[NY * zt + y], device)

    def raise_up(pair):
        for k in range(2):
            zt = 2 * pair + k
            for dy in (1, 3, 2):
                yt = around(y, dy, NY)
                wait(res.at[zt, :, lanes(yt, 128)], ry_r.at[NY * zt + yt])
        both = res[two(pair)].reshape(128, 512).astype(F32)
        fed = (both * mlp_gain[...].astype(F32).reshape(1, 512)).astype(BF16)
        part = jnp.dot(fed, wu[...], preferred_element_type=F32).astype(BF16)
        upb[two(pair)] = part.reshape(2, 64, 512)
        send(upb.at[2 * pair + 1 - c], dd.at[pair], dd_s, dd_r.at[pair], {"c": 1 - c})

    def squares():
        own = res[z, rows, :].astype(F32)
        sq2[tp] = jnp.broadcast_to(jnp.sum(own * own, axis=-1, keepdims=True), (16, 128))
        for device in tps:
            send(sq2.at[tp], sq2.at[tp], sq2_s, sq2_r, device)

    def across(pair):
        wait(dd.at[pair], dd_r.at[pair])
        us[pair] = (upb[2 * pair + c].astype(F32) + dd[pair].astype(F32)).astype(BF16)

        @pl.when(pair != x)
        def _():
            send(us.at[pair], ur.at[x], us_s, us_r.at[x], {"x": pair})

    def activate(pair):
        @pl.when(pair == x)
        def _():
            total = us[x].astype(F32)
            for dx in (1, 3, 2):
                xs = around(x, dx, NX)
                wait(ur.at[xs], us_r.at[xs])
                total = total + ur[xs].astype(F32)
            act[tp] = jnp.square(jnp.maximum(total, 0.0)).astype(BF16)
            for dx in (2, 1, 3):
                send(act.at[tp], act.at[tp], ac_s, ac_r.at[x], {"x": around(x, dx, NX)})
            send(act.at[tp], act.at[tp], ac_s, ad_r.at[x], {"c": 1 - c})

    def hand_over(pair):
        @pl.when(pair != x)
        def _():
            piece = act.at[NC * pair + c]
            wait(piece, ac_r.at[pair])
            send(piece, piece, ac_s, ad_r.at[pair], {"c": 1 - c})

    def bring_down(pair):
        wait(act.at[NC * pair + 1 - c], ad_r.at[pair])
        part = jnp.dot(act[two(pair)].reshape(128, 512), wdn[...], preferred_element_type=F32).astype(BF16)
        dp[two(pair)] = part.reshape(2, NY, 16, 512)
        for device in ys:
            send(dp.at[two(pair), device["y"]], dyb.at[y, two(pair)], dy_s, dy_r.at[pair], device)

    def settle(pair):
        wait(dyb.at[pl.ds(0, 3), two(pair)], dy_r.at[pair])
        total = dp[two(pair), y].astype(F32)
        for dy in (1, 2, 3):
            total = total + dyb[around(y, dy, NY), two(pair)].astype(F32)
        zs[two(pair)] = total.astype(BF16)
        for k in range(2):
            j = 2 * pair + k

            @pl.when(j != z)
            def _():
                send(zs.at[j], zr.at[z], zr_s, zr_r, {"z": j})

    stages = (
        (0.0, relay), (2.0, raise_up), (3.1, across), (5.2, activate), (7.3, hand_over), (8.1, bring_down), (10.5, settle),
    )
    order = sorted((offset + turn, stage, turn) for stage, (offset, _) in enumerate(stages) for turn in range(4))
    pltpu.make_async_copy(wu_hbm, wu, in_sem.at[1]).wait()
    pltpu.make_async_copy(wdn_hbm, wdn, in_sem.at[2]).wait()
    for _, stage, turn in order:
        stages[stage][1](around(first, PAIRS[turn], 4))
        if stage == 1 and turn == 0:
            squares()

    zr[z] = zs[z]
    wait(sq2.at[pl.ds(0, 7)], sq2_r)
    wait(zr.at[pl.ds(0, 7)], zr_r)
    mean = jnp.sum(sq2[...], axis=0)[:, 0:1] / D
    squared = 1.0 / (mean + EPS)
    mlp = (jnp.sum(zr[...].astype(F32), axis=0) * squared).astype(BF16).astype(F32)
    out[...] = (res[z, rows, :].astype(F32) + mlp).astype(BF16)

    wait(hx.at[pl.ds(0, 3)], hx_s)
    wait(sq.at[pl.ds(0, 7)], sq_s)
    for number in range(7):
        wait(slot(0), wo_s.at[number])
    for number, (home, array, columns) in enumerate(pieces):

        @pl.when(y != home)
        def _():
            wait(wb.at[0, :, columns], wb_s.at[number])

    for dx in range(NX):
        wait(half(hx, 0, 0), zb_s.at[2 * dx + 1])

        @pl.when(NC * around(x, dx, NX) + c != z)
        def _():
            wait(half(hx, 0, 0), zb_s.at[2 * dx])

    wait(xb.at[pl.ds(0, 28)], yb_s)

    @pl.when(y < 3)
    def _():
        wait(pb.at[pl.ds(0, 31)], rb_s)

    @pl.when(y == 3)
    def _():
        wait(pb.at[pl.ds(0, 31), :, slice(0, 256)], rb_s)

    wait(mb.at[pl.ds(0, 3)], mb_s)
    wait(hp.at[pl.ds(0, 3)], hp_s)
    wait(r2.at[pl.ds(0, 7)], op_s)
    wait(op.at[pl.ds(0, 7)], rz_s)
    wait(res.at[:, :, slice(0, 384)], ry_s)
    wait(sq2.at[pl.ds(0, 7)], sq2_s)
    wait(dd, dd_s)
    wait(us.at[pl.ds(0, 3)], us_s)
    wait(act.at[pl.ds(0, 7)], ac_s)
    wait(dyb.at[pl.ds(0, 3)], dy_s)
    wait(zr.at[pl.ds(0, 7)], zr_s)


def body(
    hidden_rows, carried_state, norm_gain, w_query, w_key, w_decay, w_value, w_gate,
    decay_bias, head_gain, w_out, mlp_gain, w_up, w_down,
):
    dma = pltpu.SemaphoreType.DMA
    vmem = pl.BlockSpec(memory_space=pltpu.VMEM)
    return pl.pallas_call(
        layer_kernel,
        out_shape=(pltpu.VMEM((16, 512), BF16), pltpu.VMEM((16, 65536), F32)),
        in_specs=[pl.BlockSpec(memory_space=pltpu.HBM)] * 14,
        out_specs=(vmem, vmem),
        scratch_shapes=[
            pltpu.VMEM((16, 512), BF16),
            pltpu.VMEM((4096,), BF16),
            pltpu.VMEM((256,), F32),
            pltpu.VMEM((256,), BF16),
            pltpu.VMEM((512,), BF16),
            pltpu.VMEM((NX, 16, 512), BF16),
            pltpu.VMEM((8, 16, 128), F32),
            pltpu.VMEM((32, 16, 512), BF16),
            pltpu.VMEM((NY, 128, 512), BF16),
            pltpu.VMEM((32, 16, 512), BF16),
            pltpu.VMEM((NY, NZ, 16, 512), BF16),
            pltpu.VMEM((16, 1792), F32),
            pltpu.VMEM((512, 1024), BF16),
            pltpu.VMEM((16, 65536), F32),
            pltpu.VMEM((16, 512), F32),
            pltpu.VMEM((16, 256), F32),
            pltpu.VMEM((512, 512), BF16),
            pltpu.VMEM((512, 512), BF16),
            pltpu.VMEM((NY, 16, 512), BF16),
            pltpu.VMEM((NY, 16, 128), BF16),
            pltpu.VMEM((8, 64, 128), BF16),
            pltpu.VMEM((8, 64, 128), BF16),
            pltpu.VMEM((NZ, 64, 512), BF16),
            pltpu.VMEM((8, 16, 128), F32),
            pltpu.VMEM((8, 64, 512), BF16),
            pltpu.VMEM((4, 64, 512), BF16),
            pltpu.VMEM((4, 64, 512), BF16),
            pltpu.VMEM((4, 64, 512), BF16),
            pltpu.VMEM((8, 64, 512), BF16),
            pltpu.VMEM((8, NY, 16, 512), BF16),
            pltpu.VMEM((NY, 8, 16, 512), BF16),
            pltpu.VMEM((8, 16, 512), BF16),
            pltpu.VMEM((NZ, 16, 512), BF16),
            dma((9,)), dma, dma((NX,)), dma, dma, dma((8,)), dma((NZ,)), dma, dma((32,)), dma((NZ,)),
            dma((5,)), dma, dma((7,)), dma((NZ,)), dma, dma((NY,)),
            dma, dma, dma, dma, dma, dma, dma, dma((NZ,)), dma, dma((32,)), dma, dma,
            dma, dma((4,)), dma, dma((4,)), dma, dma((4,)), dma((4,)), dma, dma((4,)), dma, dma,
        ],
        compiler_params=pltpu.CompilerParams(collective_id=0, has_side_effects=True, vmem_limit_bytes=(59 << 20) + (800 << 10)),
        name="layer",
    )(
        hidden_rows, norm_gain, decay_bias, head_gain, mlp_gain, w_query, w_key, w_decay, w_value, w_gate,
        w_out, w_up, w_down, carried_state,
    )


def solution(mesh):
    finer = Mesh(mesh.devices.reshape(NZ, NY, NX, NC), ("z", "y", "x", "c"))
    placed = (
        P(KV, TP), P(KV, TP), P(), P(KV, TP), P(KV, TP), P(KV, TP), P(KV, TP), P(KV, TP),
        P(TP), P(), P(TP, KV), P(TP), P(TP, KV), P(KV, TP),
    )
    return jax.shard_map(
        body, mesh=finer, in_specs=placed, out_specs=(P(KV, TP), P(KV, TP)), check_vma=False
    )
```

time: 235 us -> 90.1 us (0.38)
  Pallas kernels: 0 us -> 86.5 us
  waiting for transfers between devices: 83.7 us -> 0 us
  blocking collectives: 60.1 us -> 0 us
  starting transfers between devices: 34.3 us -> 0 us
  local copies, waits for them, and re-layouts: 20.5 us -> 2.62 us
  between operations: 14.4 us -> 0.64 us
  matrix products: 10.9 us -> 0 us
  other arithmetic: 10.3 us -> 0 us
    pallas_call x0 -> x1, Pallas kernels: none -> 86.5 us  [body(): pl.pallas_call(layer_kernel, out_shape=(pltpu.VMEM((16, 512), BF16), pltp...]
    all_to_all x6 -> x0, waiting for transfers between devices: 83.7 us -> none  [the longest x2 65.2 us: sent_and_summed(): lax.all_to_all(parts, axis, split_axis=0, concat_axis=0, tiled=True)]
    all_to_all x3 -> x0, blocking collectives: 44.3 us -> none  [the longest x1 22.3 us: sent_to_all(): return lax.all_to_all(copies, axis, split_axis=0, concat_axis=0, tiled=True)]
    all_to_all x6 -> x0, starting transfers between devices: 34.2 us -> none  [the longest x3 14.4 us: sent_to_all(): return lax.all_to_all(copies, axis, split_axis=0, concat_axis=0, tiled=True)]
    all_gather x1 -> x0, blocking collectives: 15.8 us -> none  [gather_axes(): out = lax.all_gather(out, axes[number], axis=dim, tiled=True)]
    unnamed x26 -> x2, local copies, waits for them, and re-layouts: 16.1 us -> 2.62 us
    dot_general x5 -> x0, matrix products: 10.9 us -> none  [the longest x1 4.46 us: body(): jnp.einsum('bhk,bhkv->bhv', query_heads, new_state, precision=lax.Precisi...]
    add x1 -> x0, other arithmetic: 7.22 us -> none  [body(): jnp.exp(log_decay)[..., None] * carried]
  transfers between devices with their start and end apart: 7 -> 0, of which waited for: 5 -> 0; matrix products, arithmetic and copies ran while one was open for 15% -> 0% of each run, Pallas kernels for 0% -> 0%
where the time goes in v2:
time: 90.1 us; the launch traced here: 89.8 us
  Pallas kernels  86.5 us (96%)
  local copies, waits for them, and re-layouts  2.62 us (3%)
    pallas_call x1, Pallas kernels, body(): pl.pallas_call(layer_kernel, out_shape=(pltpu.VMEM((16, 512), BF16), pltp...  86.5 us
    unnamed x2, local copies, waits for them, and re-layouts  2.62 us

profile of v2, /device:TPU:2, one launch (start us, length us, event | category | flops | bytes accessed | tf_op | source)
XLA Modules:
  0.0 89.8 jit_solution(348825951256207386)
XLA Ops:
  0.6 86.5 %layer.1 = (bf16[16,512]{1,0:T(8,128)(2,1)S(1)}, f32[16,65536]{1,0:T(8,128)S(1)}) custom-call(bf16[16,512]{1,0:T(8,128)(2,1)} %hid_hbm.1, bf16[4096]{0:T(1024)(128)(2,1)} %norm_gain_hbm.1, f32[256]{0:T(256)} %bias_hbm.1, bf16[256]{0:T(256)(128)(2,1)} %head_gain_hbm.1, bf16[512]{0:T(512)(128)(2,1)} %mlp_gain_hbm.1, bf16[128,256]{1,0:T(8,128)(2,1)} %wq.1, ...), custom_call_target="tpu_custom_call" | custom-call | tf_op jit(solution)/shard_map/layer/pallas_call | solution.py:439
  87.2 0.6 copy.18
  87.8 2.0 %copy.19 = f32[16,65536]{1,0:T(8,128)} copy(f32[16,65536]{1,0:T(8,128)S(1)} %get-tuple-element.3) | data formatting | bytes 8388608

commit v3 on v2

--- a/solution.py
+++ b/solution.py
@@ -36,10 +36,8 @@
 
 
 def greet(peers):
-    barrier = pltpu.get_barrier_semaphore()
     for device in peers:
-        pl.semaphore_signal(barrier, inc=1, device_id=device, device_id_type=MESH)
-    pl.semaphore_wait(barrier, len(peers))
+        pl.semaphore_signal(pltpu.get_barrier_semaphore(), inc=1, device_id=device, device_id_type=MESH)
 
 
 def around(index, step, count):
@@ -50,9 +48,9 @@
     hid_hbm, norm_gain_hbm, bias_hbm, head_gain_hbm, mlp_gain_hbm,
     wq, wk, wd, wv, wg, wo, wu_hbm, wdn_hbm, state_hbm,
     out, new_state, hid, norm_gain, bias, head_gain, mlp_gain,
-    hx, sq, xb, wb, pb, rb, proj, wog, state, acc, decay,
+    hx, sq, xb, wb, pb, rb, rl, proj, wog, state, acc, decay, asked,
     wu, wdn, mb, hp, op, r2, res, sq2, upb, dd, us, ur, act, dp, dyb, zs, zr,
-    in_sem, hx_s, hx_r, sq_s, sq_r, zb_s, zb_r, yb_s, yb_r, db_r, wb_s, wb_r, wo_s, wo_r, rb_s, rb_r,
+    in_sem, hx_s, hx_r, sq_s, sq_r, zb_s, zb_r, yb_s, yb_r, db_r, wb_s, wb_r, wo_s, wo_r, rb_s, rb_r, rl_s, rl_r,
     mb_s, mb_r, hp_s, hp_r, op_s, op_r, rz_s, rz_r, ry_s, ry_r, sq2_s, sq2_r,
     dd_s, dd_r, us_s, us_r, ac_s, ac_r, ad_r, dy_s, dy_r, zr_s, zr_r,
 ):
@@ -67,33 +65,43 @@
     pltpu.make_async_copy(state_hbm, state, in_sem.at[0]).start()
     pltpu.make_async_copy(wu_hbm, wu, in_sem.at[1]).start()
     pltpu.make_async_copy(wdn_hbm, wdn, in_sem.at[2]).start()
+    tps = [
+        {"x": around(x, dx, NX), "c": around(c, dc, NC)} for dx in (2, 1, 3, 0) for dc in range(NC) if dx or dc
+    ]
+    ys = [{"y": around(y, dy, NY)} for dy in (2, 1, 3)]
+    zfar = [{"z": around(z, dz, NZ)} for dz in (4, 3, 5, 2, 6, 1, 7)]
+    peers = tps + zfar + [{"z": device["z"], "c": 1 - c} for device in zfar] + ys
+    greet(peers)
     for number, (src, dst) in enumerate(small):
         pltpu.make_async_copy(src, dst, in_sem.at[4 + number]).wait()
     h = hid[...].astype(F32)
     gain = norm_gain[pl.ds(pl.multiple_of(tp * 512, 512), 512)].astype(F32).reshape(1, 512)
     hx[x] = (h * gain).astype(BF16)
     sq[tp] = jnp.broadcast_to(jnp.sum(h * h, axis=-1, keepdims=True), (16, 128))
-    tps = [
-        {"x": around(x, dx, NX), "c": around(c, dc, NC)} for dx in (2, 1, 3, 0) for dc in range(NC) if dx or dc
-    ]
-    ys = [{"y": around(y, dy, NY)} for dy in (2, 1, 3)]
-    zfar = [{"z": around(z, dz, NZ)} for dz in (4, 3, 5, 2, 6, 1, 7)]
-    greet(tps + zfar + [{"z": device["z"], "c": 1 - c} for device in zfar] + ys)
+    pl.semaphore_wait(pltpu.get_barrier_semaphore(), len(peers))
 
     def lanes(index, width):
         return pl.ds(pl.multiple_of(index * width, width), width)
 
-    def slot(origin):
-        return wog.at[:, lanes(origin, 128)]
+    side = 1 - 2 * c
+
+    def at(offset):
+        return lax.rem(z + offset * side + NZ, NZ)
+
+    def slot(origin, part):
+        return wog.at[pl.ds(part * 256, 256), lanes(origin, 128)]
 
     for dx in (2, 1, 3):
         send(hx.at[x], hx.at[x], hx_s, hx_r.at[x], {"x": around(x, dx, NX)})
     for device in tps:
         send(sq.at[tp], sq.at[tp], sq_s, sq_r, device)
     up, down = around(z, 1, NZ), around(z, NZ - 1, NZ)
-    send(wo, slot(z), wo_s.at[0], wo_r.at[z], {"z": up})
-    send(wo, slot(z), wo_s.at[1], wo_r.at[z], {"z": down})
-    pltpu.make_async_copy(wo, slot(z), in_sem.at[3]).start()
+    for part in range(2):
+        mine = wo.at[pl.ds(part * 256, 256)]
+        send(mine, slot(z, part), wo_s.at[7 * part], wo_r.at[part, z], {"z": up})
+        send(mine, slot(z, part), wo_s.at[7 * part + 1], wo_r.at[part, z], {"z": down})
+    own_out = pltpu.make_async_copy(wo, wog.at[:, lanes(z, 128)], in_sem.at[3])
+    own_out.start()
     pieces = (
         (0, wv, slice(0, 512)),
         (1, wg, slice(0, 512)),
@@ -117,14 +125,14 @@
         send(hid.at[:, lanes(yt, 128)], hp.at[y], hp_s, hp_r, {"y": yt})
     hp[y] = hid[:, lanes(y, 128)]
 
-    def pass_on(step):
+    def pass_on(step, part):
         low = around(z, NZ - step + 1, NZ)
-        wait(slot(low), wo_r.at[low])
-        send(slot(low), slot(low), wo_s.at[2 * step - 2], wo_r.at[low], {"z": up})
+        wait(slot(low, part), wo_r.at[part, low])
+        send(slot(low, part), slot(low, part), wo_s.at[7 * part + 2 * step - 2], wo_r.at[part, low], {"z": up})
         high = around(z, step - 1, NZ)
-        wait(slot(high), wo_r.at[high])
+        wait(slot(high, part), wo_r.at[part, high])
         if step < 4:
-            send(slot(high), slot(high), wo_s.at[2 * step - 1], wo_r.at[high], {"z": down})
+            send(slot(high, part), slot(high, part), wo_s.at[7 * part + 2 * step - 1], wo_r.at[part, high], {"z": down})
 
     def half(ref, number, which):
         return ref.at[number, :, lanes(which, 256)]
@@ -135,15 +143,15 @@
             wait(hx.at[xs], hx_r.at[xs])
         zt = NC * xs + c
         for dc in range(NC):
-            side = around(c, dc, NC)
-            src, dst = half(hx, xs, side), half(xb, kv, side)
+            core = around(c, dc, NC)
+            src, dst = half(hx, xs, core), half(xb, kv, core)
             if dc:
-                send(src, dst, zb_s.at[2 * dx + dc], zb_r.at[z], {"z": zt, "c": side})
+                send(src, dst, zb_s.at[2 * dx + dc], zb_r.at[z], {"z": zt, "c": core})
             else:
 
                 @pl.when(zt != z)
                 def _():
-                    send(src, dst, zb_s.at[2 * dx], zb_r.at[z], {"z": zt, "c": side})
+                    send(src, dst, zb_s.at[2 * dx], zb_r.at[z], {"z": zt, "c": core})
 
                 @pl.when(zt == z)
                 def _():
@@ -151,7 +159,7 @@
 
     def spread_y(group):
         for dz in group:
-            zt = around(z, dz, NZ)
+            zt = at(dz)
             number = NY * zt + y
             piece = half(xb, number, c)
             wait(piece, zb_r.at[zt])
@@ -161,65 +169,79 @@
 
     def spread_c(group):
         for dz in group:
-            zt = around(z, dz, NZ)
+            zt = at(dz)
             for dy in (1, 3, 2):
                 number = NY * zt + around(y, dy, NY)
                 piece = half(xb, number, c)
                 wait(piece, yb_r.at[number])
                 send(piece, piece, yb_s, db_r.at[zt], {"c": 1 - c})
 
-    def scatter(steps, width):
-        for dz in steps:
-            zt = around(z, dz, NZ)
-            for dy in (2, 1, 3, 0):
-                yt = around(y, dy, NY)
-                src = pb.at[NY * zt + yt, :, slice(0, width)]
-                dst = rb.at[y, z, :, slice(0, width)]
-                if dz or dy:
-                    send(src, dst, rb_s, rb_r.at[y], {"z": zt, "y": yt})
-                else:
-                    pltpu.make_async_copy(src, dst, rb_r.at[y]).start()
+    def plane(offset):
+        return pl.ds(pl.multiple_of(NY * at(offset), NY), NY)
+
+    def by_width(action):
+        @pl.when(y < 3)
+        def _():
+            action(512)
+
+        @pl.when(y == 3)
+        def _():
+            action(256)
+
+    def scatter(offset, kind, width):
+        for dy in (2, 1, 3, 0):
+            yt = around(y, dy, NY)
+            src = pb.at[NY * at(offset) + yt, :, slice(0, width)]
+            dst = rb.at[y, kind, :, slice(0, width)]
+            if offset or dy:
+                send(src, dst, rb_s, rb_r.at[y], {"z": at(offset), "y": yt})
+            else:
+                pltpu.make_async_copy(src, dst, rb_r.at[y]).start()
+
+    def lend(offset, number, via, width):
+        src, dst = pb.at[plane(offset), :, slice(0, width)], rl.at[number, :, :, slice(0, width)]
+        send(src, dst, rl_s, rl_r.at[number], {"z": at(via)})
+
+    def combine(offset, number, kind, width):
+        wait(rl.at[number, :, :, slice(0, width)], rl_r.at[number])
+        total = pb[plane(offset), :, 0:width].astype(F32) + rl[number, :, :, 0:width].astype(F32)
+        pb[plane(offset), :, 0:width] = total.astype(BF16)
+        scatter(offset, kind, width)
 
     def multiply(group):
         for dz in group:
-            zt = around(z, dz, NZ)
-            wait(xb.at[pl.ds(pl.multiple_of(NY * zt, NY), NY), :, slice(0, 256)], db_r.at[zt])
-        rows = [xb[pl.ds(pl.multiple_of(NY * around(z, dz, NZ), NY), NY)].reshape(64, 512) for dz in group]
+            wait(xb.at[plane(dz), :, slice(0, 256)], db_r.at[at(dz)])
+        rows = [xb[plane(dz)].reshape(64, 512) for dz in group]
         weights = wb[...].reshape(512, 512)
         part = jnp.dot(jnp.concatenate(rows, axis=0), weights, preferred_element_type=F32).astype(BF16)
         for number, dz in enumerate(group):
-            zt = around(z, dz, NZ)
-            pb[pl.ds(pl.multiple_of(NY * zt, NY), NY)] = part[64 * number : 64 * number + 64].reshape(NY, 16, 512)
-
-        @pl.when(y < 3)
-        def _():
-            scatter(group, 512)
-
-        @pl.when(y == 3)
-        def _():
-            scatter(group, 256)
-
-    for group in GROUPS:
-        spread_y(group)
+            pb[plane(dz)] = part[64 * number : 64 * number + 64].reshape(NY, 16, 512)
+
+    spread_y(GROUPS[0])
+    pass_on(2, 0)
+    spread_y(GROUPS[1])
+    pass_on(2, 1)
+    spread_y(GROUPS[2])
+    spread_y(GROUPS[3])
     spread_c(GROUPS[0])
+    pass_on(3, 0)
     spread_c(GROUPS[1])
-    pass_on(2)
-
-    @pl.when(y < 3)
-    def _():
-        wait(wb, wb_r)
-
-    @pl.when(y == 3)
-    def _():
-        wait(wb.at[:, :, slice(0, 256)], wb_r)
-
+    pass_on(3, 1)
+    by_width(lambda width: wait(wb.at[:, :, slice(0, width)], wb_r))
     multiply(GROUPS[0])
     spread_c(GROUPS[2])
+    by_width(lambda width: scatter(0, 0, width))
     multiply(GROUPS[1])
     spread_c(GROUPS[3])
+    by_width(lambda width: (lend(2, 0, 1, width), scatter(7, 4, width)))
+    multiply(GROUPS[3])
+    by_width(lambda width: (lend(4, 1, 1, width), lend(5, 2, 7, width)))
     multiply(GROUPS[2])
-    multiply(GROUPS[3])
-    pass_on(3)
+    by_width(lambda width: combine(1, 0, 1, width))
+    pass_on(4, 0)
+    by_width(lambda width: combine(3, 1, 2, width))
+    by_width(lambda width: combine(6, 2, 3, width))
+    pass_on(4, 1)
 
     wait(sq.at[pl.ds(0, 7)], sq_r)
     scale = lax.rsqrt(jnp.sum(sq[...], axis=0) / D + EPS)[:, 0:1]
@@ -237,24 +259,36 @@
     soft = jnp.minimum(pre, 0.0) - jnp.log1p(jnp.exp(-jnp.abs(pre)))
     decay[...] = jnp.exp(soft / 16.0)
     acc[...] = jnp.zeros_like(acc)
+    queries, keys_now = proj[:, 256:512] * DK ** (-0.5), proj[:, 512:768]
+    asked[...] = queries * decay[...]
+    for head in range(2):
+        columns = slice(head * DK, head * DK + DK)
+        meet = jnp.sum(queries[:, columns] * keys_now[:, columns], axis=-1, keepdims=True)
+        acc[:, head * DV : head * DV + DV] = meet * proj[:, 768 + head * DV : 768 + head * DV + DV]
     pltpu.make_async_copy(state_hbm, state, in_sem.at[0]).wait()
+
+    def turned(ref, step):
+        return pltpu.roll(ref, lax.rem(256 - step * KEYS, 256), axis=1)
 
     @pl.loop(0, 256 // KEYS)
     def _(step):
-        shift = lax.rem(256 - step * KEYS, 256)
-        rates = pltpu.roll(decay[...], shift, axis=1)
-        queries = pltpu.roll(proj[:, 256:512] * DK ** (-0.5), shift, axis=1)
-        keys = pltpu.roll(proj[:, 512:768], shift, axis=1)
-        head = step // (DK // KEYS)
-        columns = lanes(head, DV)
-        values = proj[:, pl.ds(pl.multiple_of(768 + head * DV, DV), DV)]
-        total = acc[:, columns]
+        weights = turned(asked[...], step)
+        columns = lanes(step // (DK // KEYS), DV)
+        totals = [acc[:, columns], jnp.zeros((16, DV), F32)]
         for key in range(KEYS):
             where = pl.ds(pl.multiple_of((step * KEYS + key) * DV, DV), DV)
-            fresh = rates[:, key : key + 1] * state[:, where] + keys[:, key : key + 1] * values
-            new_state[:, where] = fresh
-            total = total + queries[:, key : key + 1] * fresh
-        acc[:, columns] = total
+            totals[key % 2] = totals[key % 2] + weights[:, key : key + 1] * state[:, where]
+        acc[:, columns] = totals[0] + totals[1]
+
+    def renew(first_step, steps):
+        @pl.loop(first_step, first_step + steps)
+        def _(step):
+            rates = turned(decay[...], step)
+            keys = turned(proj[:, 512:768], step)
+            values = proj[:, pl.ds(pl.multiple_of(768 + step // (DK // KEYS) * DV, DV), DV)]
+            for key in range(KEYS):
+                where = pl.ds(pl.multiple_of((step * KEYS + key) * DV, DV), DV)
+                new_state[:, where] = rates[:, key : key + 1] * state[:, where] + keys[:, key : key + 1] * values
 
     for number in range(2):
         part = slice(number * DV, number * DV + DV)
@@ -265,11 +299,12 @@
         mb[y, :, part] = (normal * head_gain[...].astype(F32).reshape(1, DV) * silu).astype(BF16)
     for device in ys:
         send(mb.at[y], mb.at[y], mb_s, mb_r, device)
-    pass_on(4)
+    renew(0, 2)
     here = lanes(y, 128)
     last = around(z, 4, NZ)
-    wait(slot(last), wo_r.at[last])
-    pltpu.make_async_copy(wo, slot(z), in_sem.at[3]).wait()
+    for part in range(2):
+        wait(slot(last, part), wo_r.at[part, last])
+    own_out.wait()
     wait(mb.at[pl.ds(0, 3)], mb_r)
     part = jnp.dot(mb[...].reshape(64, 512), wog[...], preferred_element_type=F32).astype(BF16)
     for t in range(8):
@@ -278,18 +313,20 @@
     for device in tps:
         t = NC * device["x"] + device["c"]
         send(op.at[t], r2.at[tp], op_s, op_r, device)
+    renew(2, 2)
     wait(hp.at[pl.ds(0, 3)], hp_r)
     wait(r2.at[pl.ds(0, 7)], op_r)
     attn = jnp.sum(r2[...].astype(F32), axis=0).astype(BF16).astype(F32)
     res[z, :, here] = (hp[...].reshape(64, 128).astype(F32) + attn).astype(BF16)
     mine = res.at[z, :, here]
-    for device in zfar:
+    for device in zfar[::-1]:
         send(mine, mine, rz_s, rz_r.at[z], device)
     for device in ys:
         send(mine, mine, ry_s, ry_r.at[kv], device)
 
     rows = pl.ds(pl.multiple_of(y * 16, 16), 16)
     first = z // 2
+    lean = 2 * (z % 2) - 1
 
     def two(pair):
         return pl.ds(pl.multiple_of(2 * pair, 2), 2)
@@ -378,9 +415,11 @@
     pltpu.make_async_copy(wu_hbm, wu, in_sem.at[1]).wait()
     pltpu.make_async_copy(wdn_hbm, wdn, in_sem.at[2]).wait()
     for _, stage, turn in order:
-        stages[stage][1](around(first, PAIRS[turn], 4))
+        stages[stage][1](lax.rem(first + lean * PAIRS[turn] + 4, 4))
         if stage == 1 and turn == 0:
             squares()
+        if stage == 2 and turn >= 2:
+            renew(2 * turn, 2)
 
     zr[z] = zs[z]
     wait(sq2.at[pl.ds(0, 7)], sq2_r)
@@ -392,8 +431,8 @@
 
     wait(hx.at[pl.ds(0, 3)], hx_s)
     wait(sq.at[pl.ds(0, 7)], sq_s)
-    for number in range(7):
-        wait(slot(0), wo_s.at[number])
+    for number in range(14):
+        wait(slot(0, 0), wo_s.at[number])
     for number, (home, array, columns) in enumerate(pieces):
 
         @pl.when(y != home)
@@ -409,13 +448,8 @@
 
     wait(xb.at[pl.ds(0, 28)], yb_s)
 
-    @pl.when(y < 3)
-    def _():
-        wait(pb.at[pl.ds(0, 31)], rb_s)
-
-    @pl.when(y == 3)
-    def _():
-        wait(pb.at[pl.ds(0, 31), :, slice(0, 256)], rb_s)
+    by_width(lambda width: wait(pb.at[pl.ds(0, 19), :, slice(0, width)], rb_s))
+    by_width(lambda width: wait(pb.at[pl.ds(0, 12), :, slice(0, width)], rl_s))
 
     wait(mb.at[pl.ds(0, 3)], mb_s)
     wait(hp.at[pl.ds(0, 3)], hp_s)
@@ -452,11 +486,13 @@
             pltpu.VMEM((32, 16, 512), BF16),
             pltpu.VMEM((NY, 128, 512), BF16),
             pltpu.VMEM((32, 16, 512), BF16),
-            pltpu.VMEM((NY, NZ, 16, 512), BF16),
+            pltpu.VMEM((NY, 5, 16, 512), BF16),
+            pltpu.VMEM((3, NY, 16, 512), BF16),
             pltpu.VMEM((16, 1792), F32),
             pltpu.VMEM((512, 1024), BF16),
             pltpu.VMEM((16, 65536), F32),
             pltpu.VMEM((16, 512), F32),
+            pltpu.VMEM((16, 256), F32),
             pltpu.VMEM((16, 256), F32),
             pltpu.VMEM((512, 512), BF16),
             pltpu.VMEM((512, 512), BF16),
@@ -476,7 +512,7 @@
             pltpu.VMEM((8, 16, 512), BF16),
             pltpu.VMEM((NZ, 16, 512), BF16),
             dma((9,)), dma, dma((NX,)), dma, dma, dma((8,)), dma((NZ,)), dma, dma((32,)), dma((NZ,)),
-            dma((5,)), dma, dma((7,)), dma((NZ,)), dma, dma((NY,)),
+            dma((5,)), dma, dma((14,)), dma((2, NZ)), dma, dma((NY,)), dma, dma((3,)),
             dma, dma, dma, dma, dma, dma, dma, dma((NZ,)), dma, dma((32,)), dma, dma,
             dma, dma((4,)), dma, dma((4,)), dma, dma((4,)), dma((4,)), dma, dma((4,)), dma, dma,
         ],

time: 90.1 us -> 84.4 us (0.937)
  Pallas kernels: 86.5 us -> 81 us
    pallas_call x1, Pallas kernels: 86.5 us -> 81 us  [body(): pl.pallas_call(layer_kernel, out_shape=(pltpu.VMEM((16, 512), BF16), pltp...]
where the time goes in v3:
time: 84.4 us; the launch traced here: 84.3 us
  Pallas kernels  81 us (96%)
  local copies, waits for them, and re-layouts  2.62 us (3%)
    pallas_call x1, Pallas kernels, body(): pl.pallas_call(layer_kernel, out_shape=(pltpu.VMEM((16, 512), BF16), pltp...  81 us
    unnamed x2, local copies, waits for them, and re-layouts  2.62 us

profile of v3, /device:TPU:2, one launch (start us, length us, event | category | flops | bytes accessed | tf_op | source)
XLA Modules:
  0.0 84.3 jit_solution(3500966032368901762)
XLA Ops:
  0.6 81.0 %layer.1 = (bf16[16,512]{1,0:T(8,128)(2,1)S(1)}, f32[16,65536]{1,0:T(8,128)S(1)}) custom-call(bf16[16,512]{1,0:T(8,128)(2,1)} %hid_hbm.1, bf16[4096]{0:T(1024)(128)(2,1)} %norm_gain_hbm.1, f32[256]{0:T(256)} %bias_hbm.1, bf16[256]{0:T(256)(128)(2,1)} %head_gain_hbm.1, bf16[512]{0:T(512)(128)(2,1)} %mlp_gain_hbm.1, bf16[128,256]{1,0:T(8,128)(2,1)} %wq.1, ...), custom_call_target="tpu_custom_call" | custom-call | tf_op jit(solution)/shard_map/layer/pallas_call | solution.py:473
  81.7 0.6 copy.18
  82.3 2.0 %copy.19 = f32[16,65536]{1,0:T(8,128)} copy(f32[16,65536]{1,0:T(8,128)S(1)} %get-tuple-element.3) | data formatting | bytes 8388608

commit v4 on v3

--- a/solution.py
+++ b/solution.py
@@ -270,15 +270,13 @@
     def turned(ref, step):
         return pltpu.roll(ref, lax.rem(256 - step * KEYS, 256), axis=1)
 
-    @pl.loop(0, 256 // KEYS)
-    def _(step):
-        weights = turned(asked[...], step)
-        columns = lanes(step // (DK // KEYS), DV)
-        totals = [acc[:, columns], jnp.zeros((16, DV), F32)]
-        for key in range(KEYS):
-            where = pl.ds(pl.multiple_of((step * KEYS + key) * DV, DV), DV)
-            totals[key % 2] = totals[key % 2] + weights[:, key : key + 1] * state[:, where]
-        acc[:, columns] = totals[0] + totals[1]
+    for head in range(2):
+        columns = slice(head * DV, head * DV + DV)
+        totals = [acc[:, columns]] + [jnp.zeros((16, DV), F32)] * 3
+        for key in range(head * DK, head * DK + DK):
+            weight = asked[:, key : key + 1]
+            totals[key % 4] = totals[key % 4] + weight * state[:, key * DV : key * DV + DV]
+        acc[:, columns] = (totals[0] + totals[1]) + (totals[2] + totals[3])
 
     def renew(first_step, steps):
         @pl.loop(first_step, first_step + steps)
@@ -299,7 +297,7 @@
         mb[y, :, part] = (normal * head_gain[...].astype(F32).reshape(1, DV) * silu).astype(BF16)
     for device in ys:
         send(mb.at[y], mb.at[y], mb_s, mb_r, device)
-    renew(0, 2)
+    renew(0, 4)
     here = lanes(y, 128)
     last = around(z, 4, NZ)
     for part in range(2):
@@ -313,20 +311,21 @@
     for device in tps:
         t = NC * device["x"] + device["c"]
         send(op.at[t], r2.at[tp], op_s, op_r, device)
-    renew(2, 2)
+    renew(4, 4)
     wait(hp.at[pl.ds(0, 3)], hp_r)
     wait(r2.at[pl.ds(0, 7)], op_r)
     attn = jnp.sum(r2[...].astype(F32), axis=0).astype(BF16).astype(F32)
     res[z, :, here] = (hp[...].reshape(64, 128).astype(F32) + attn).astype(BF16)
     mine = res.at[z, :, here]
-    for device in zfar[::-1]:
-        send(mine, mine, rz_s, rz_r.at[z], device)
+    first = z // 2
+    lean = 2 * (z % 2) - 1
+    pairs = [lax.rem(first + lean * turn + 4, 4) for turn in PAIRS]
+    for zt in [z - lean] + [2 * pair + k for pair in pairs[1:] for k in range(2)]:
+        send(mine, mine, rz_s, rz_r.at[z], {"z": zt})
     for device in ys:
         send(mine, mine, ry_s, ry_r.at[kv], device)
 
     rows = pl.ds(pl.multiple_of(y * 16, 16), 16)
-    first = z // 2
-    lean = 2 * (z % 2) - 1
 
     def two(pair):
         return pl.ds(pl.multiple_of(2 * pair, 2), 2)
@@ -362,31 +361,26 @@
 
     def across(pair):
         wait(dd.at[pair], dd_r.at[pair])
-        us[pair] = (upb[2 * pair + c].astype(F32) + dd[pair].astype(F32)).astype(BF16)
-
-        @pl.when(pair != x)
-        def _():
-            send(us.at[pair], ur.at[x], us_s, us_r.at[x], {"x": pair})
+        total = upb[2 * pair + c].astype(F32) + dd[pair].astype(F32)
+        us[pair] = total.astype(BF16).reshape(NX, 16, 512)
+        for dx in (2, 1, 3):
+            xs = around(x, dx, NX)
+            send(us.at[pair, xs], ur.at[pair, x], us_s, us_r.at[pair], {"x": xs})
 
     def activate(pair):
-        @pl.when(pair == x)
-        def _():
-            total = us[x].astype(F32)
-            for dx in (1, 3, 2):
-                xs = around(x, dx, NX)
-                wait(ur.at[xs], us_r.at[xs])
-                total = total + ur[xs].astype(F32)
-            act[tp] = jnp.square(jnp.maximum(total, 0.0)).astype(BF16)
-            for dx in (2, 1, 3):
-                send(act.at[tp], act.at[tp], ac_s, ac_r.at[x], {"x": around(x, dx, NX)})
-            send(act.at[tp], act.at[tp], ac_s, ad_r.at[x], {"c": 1 - c})
+        wait(ur.at[pair, pl.ds(0, 3)], us_r.at[pair])
+        total = us[pair, x].astype(F32)
+        for dx in (1, 3, 2):
+            total = total + ur[pair, around(x, dx, NX)].astype(F32)
+        act[2 * pair + c, x] = jnp.square(jnp.maximum(total, 0.0)).astype(BF16)
+        piece = act.at[2 * pair + c, x]
+        for dx in (2, 1, 3):
+            send(piece, piece, ac_s, ac_r.at[pair], {"x": around(x, dx, NX)})
 
     def hand_over(pair):
-        @pl.when(pair != x)
-        def _():
-            piece = act.at[NC * pair + c]
-            wait(piece, ac_r.at[pair])
-            send(piece, piece, ac_s, ad_r.at[pair], {"c": 1 - c})
+        piece = act.at[2 * pair + c]
+        wait(piece.at[pl.ds(0, 3)], ac_r.at[pair])
+        send(piece, piece, ac_s, ad_r.at[pair], {"c": 1 - c})
 
     def bring_down(pair):
         wait(act.at[NC * pair + 1 - c], ad_r.at[pair])
@@ -409,17 +403,15 @@
                 send(zs.at[j], zr.at[z], zr_s, zr_r, {"z": j})
 
     stages = (
-        (0.0, relay), (2.0, raise_up), (3.1, across), (5.2, activate), (7.3, hand_over), (8.1, bring_down), (10.5, settle),
+        (0.0, relay), (2.0, raise_up), (3.1, across), (5.2, activate), (7.3, hand_over), (8.4, bring_down), (10.5, settle),
     )
     order = sorted((offset + turn, stage, turn) for stage, (offset, _) in enumerate(stages) for turn in range(4))
     pltpu.make_async_copy(wu_hbm, wu, in_sem.at[1]).wait()
     pltpu.make_async_copy(wdn_hbm, wdn, in_sem.at[2]).wait()
     for _, stage, turn in order:
-        stages[stage][1](lax.rem(first + lean * PAIRS[turn] + 4, 4))
+        stages[stage][1](pairs[turn])
         if stage == 1 and turn == 0:
             squares()
-        if stage == 2 and turn >= 2:
-            renew(2 * turn, 2)
 
     zr[z] = zs[z]
     wait(sq2.at[pl.ds(0, 7)], sq2_r)
@@ -504,9 +496,9 @@
             pltpu.VMEM((8, 16, 128), F32),
             pltpu.VMEM((8, 64, 512), BF16),
             pltpu.VMEM((4, 64, 512), BF16),
-            pltpu.VMEM((4, 64, 512), BF16),
-            pltpu.VMEM((4, 64, 512), BF16),
-            pltpu.VMEM((8, 64, 512), BF16),
+            pltpu.VMEM((4, NX, 16, 512), BF16),
+            pltpu.VMEM((4, NX, 16, 512), BF16),
+            pltpu.VMEM((8, NX, 16, 512), BF16),
             pltpu.VMEM((8, NY, 16, 512), BF16),
             pltpu.VMEM((NY, 8, 16, 512), BF16),
             pltpu.VMEM((8, 16, 512), BF16),

time: 84.4 us -> 80.3 us (0.951)
  Pallas kernels: 81 us -> 76.7 us
    pallas_call x1, Pallas kernels: 81 us -> 76.7 us  [body(): pl.pallas_call(layer_kernel, out_shape=(pltpu.VMEM((16, 512), BF16), pltp...]
where the time goes in v4:
time: 80.3 us; the launch traced here: 79.9 us
  Pallas kernels  76.7 us (96%)
  local copies, waits for them, and re-layouts  2.62 us (3%)
    pallas_call x1, Pallas kernels, body(): pl.pallas_call(layer_kernel, out_shape=(pltpu.VMEM((16, 512), BF16), pltp...  76.7 us
    unnamed x2, local copies, waits for them, and re-layouts  2.62 us

profile of v4, /device:TPU:2, one launch (start us, length us, event | category | flops | bytes accessed | tf_op | source)
XLA Modules:
  0.0 79.9 jit_solution(10772535491312000255)
XLA Ops:
  0.6 76.7 %layer.1 = (bf16[16,512]{1,0:T(8,128)(2,1)S(1)}, f32[16,65536]{1,0:T(8,128)S(1)}) custom-call(bf16[16,512]{1,0:T(8,128)(2,1)} %hid_hbm.1, bf16[4096]{0:T(1024)(128)(2,1)} %norm_gain_hbm.1, f32[256]{0:T(256)} %bias_hbm.1, bf16[256]{0:T(256)(128)(2,1)} %head_gain_hbm.1, bf16[512]{0:T(512)(128)(2,1)} %mlp_gain_hbm.1, bf16[128,256]{1,0:T(8,128)(2,1)} %wq.1, ...), custom_call_target="tpu_custom_call" | custom-call | tf_op jit(solution)/shard_map/layer/pallas_call | solution.py:465
  77.3 0.6 copy.18
  77.9 2.0 %copy.19 = f32[16,65536]{1,0:T(8,128)} copy(f32[16,65536]{1,0:T(8,128)S(1)} %get-tuple-element.3) | data formatting | bytes 8388608

commit v5 on v4

--- a/solution.py
+++ b/solution.py
@@ -17,7 +17,7 @@
 TP = ("x", "c")
 NZ, NY, NX, NC = 8, 4, 4, 2
 GROUPS = ((0, 1), (7, 2), (6, 3), (5, 4))
-PAIRS = (0, 1, 3, 2)
+PAIRS = (0, 1, 2, 3)
 KEYS = 32
 
 
@@ -233,14 +233,14 @@
     by_width(lambda width: scatter(0, 0, width))
     multiply(GROUPS[1])
     spread_c(GROUPS[3])
-    by_width(lambda width: (lend(2, 0, 1, width), scatter(7, 4, width)))
+    by_width(lambda width: lend(2, 0, 1, width))
     multiply(GROUPS[3])
-    by_width(lambda width: (lend(4, 1, 1, width), lend(5, 2, 7, width)))
+    by_width(lambda width: (lend(4, 1, 1, width), lend(5, 2, 7, width), scatter(7, 4, width)))
     multiply(GROUPS[2])
     by_width(lambda width: combine(1, 0, 1, width))
-    pass_on(4, 0)
     by_width(lambda width: combine(3, 1, 2, width))
     by_width(lambda width: combine(6, 2, 3, width))
+    pass_on(4, 0)
     pass_on(4, 1)
 
     wait(sq.at[pl.ds(0, 7)], sq_r)
@@ -297,7 +297,6 @@
         mb[y, :, part] = (normal * head_gain[...].astype(F32).reshape(1, DV) * silu).astype(BF16)
     for device in ys:
         send(mb.at[y], mb.at[y], mb_s, mb_r, device)
-    renew(0, 4)
     here = lanes(y, 128)
     last = around(z, 4, NZ)
     for part in range(2):
@@ -311,7 +310,6 @@
     for device in tps:
         t = NC * device["x"] + device["c"]
         send(op.at[t], r2.at[tp], op_s, op_r, device)
-    renew(4, 4)
     wait(hp.at[pl.ds(0, 3)], hp_r)
     wait(r2.at[pl.ds(0, 7)], op_r)
     attn = jnp.sum(r2[...].astype(F32), axis=0).astype(BF16).astype(F32)
@@ -405,15 +403,19 @@
     stages = (
         (0.0, relay), (2.0, raise_up), (3.1, across), (5.2, activate), (7.3, hand_over), (8.4, bring_down), (10.5, settle),
     )
+    gaps = [(5, 1), (5, 2), (6, 2), (6, 3)]
     order = sorted((offset + turn, stage, turn) for stage, (offset, _) in enumerate(stages) for turn in range(4))
     pltpu.make_async_copy(wu_hbm, wu, in_sem.at[1]).wait()
     pltpu.make_async_copy(wdn_hbm, wdn, in_sem.at[2]).wait()
     for _, stage, turn in order:
+        if (stage, turn) in gaps:
+            renew(gaps.index((stage, turn)), 1)
         stages[stage][1](pairs[turn])
         if stage == 1 and turn == 0:
             squares()
 
     zr[z] = zs[z]
+    renew(4, 4)
     wait(sq2.at[pl.ds(0, 7)], sq2_r)
     wait(zr.at[pl.ds(0, 7)], zr_r)
     mean = jnp.sum(sq2[...], axis=0)[:, 0:1] / D

time: 80.3 us -> 79.1 us (0.985)
  Pallas kernels: 76.7 us -> 75.6 us
    pallas_call x1, Pallas kernels: 76.7 us -> 75.6 us  [body(): pl.pallas_call(layer_kernel, out_shape=(pltpu.VMEM((16, 512), BF16), pltp...]
where the time goes in v5:
time: 79.1 us; the launch traced here: 78.9 us
  Pallas kernels  75.6 us (96%)
  local copies, waits for them, and re-layouts  2.62 us (3%)
    pallas_call x1, Pallas kernels, body(): pl.pallas_call(layer_kernel, out_shape=(pltpu.VMEM((16, 512), BF16), pltp...  75.6 us
    unnamed x2, local copies, waits for them, and re-layouts  2.62 us

profile of v5, /device:TPU:2, one launch (start us, length us, event | category | flops | bytes accessed | tf_op | source)
XLA Modules:
  0.0 78.9 jit_solution(14828723826458066928)
XLA Ops:
  0.6 75.6 %layer.1 = (bf16[16,512]{1,0:T(8,128)(2,1)S(1)}, f32[16,65536]{1,0:T(8,128)S(1)}) custom-call(bf16[16,512]{1,0:T(8,128)(2,1)} %hid_hbm.1, bf16[4096]{0:T(1024)(128)(2,1)} %norm_gain_hbm.1, f32[256]{0:T(256)} %bias_hbm.1, bf16[256]{0:T(256)(128)(2,1)} %head_gain_hbm.1, bf16[512]{0:T(512)(128)(2,1)} %mlp_gain_hbm.1, bf16[128,256]{1,0:T(8,128)(2,1)} %wq.1, ...), custom_call_target="tpu_custom_call" | custom-call | tf_op jit(solution)/shard_map/layer/pallas_call | solution.py:467
  76.3 0.6 copy.18
  76.9 2.0 %copy.19 = f32[16,65536]{1,0:T(8,128)} copy(f32[16,65536]{1,0:T(8,128)S(1)} %get-tuple-element.3) | data formatting | bytes 8388608

commit v6 on v5

--- a/solution.py
+++ b/solution.py
@@ -49,10 +49,10 @@
     wq, wk, wd, wv, wg, wo, wu_hbm, wdn_hbm, state_hbm,
     out, new_state, hid, norm_gain, bias, head_gain, mlp_gain,
     hx, sq, xb, wb, pb, rb, rl, proj, wog, state, acc, decay, asked,
-    wu, wdn, mb, hp, op, r2, res, sq2, upb, dd, us, ur, act, dp, dyb, zs, zr,
+    wu, wdn, mb, hp, op, r2, res, sq2, upb, ur, act, dp, dyb, zs, zr,
     in_sem, hx_s, hx_r, sq_s, sq_r, zb_s, zb_r, yb_s, yb_r, db_r, wb_s, wb_r, wo_s, wo_r, rb_s, rb_r, rl_s, rl_r,
     mb_s, mb_r, hp_s, hp_r, op_s, op_r, rz_s, rz_r, ry_s, ry_r, sq2_s, sq2_r,
-    dd_s, dd_r, us_s, us_r, ac_s, ac_r, ad_r, dy_s, dy_r, zr_s, zr_r,
+    us_s, us_r, ac_s, ac_r, ad_r, dy_s, dy_r, zr_s, zr_r,
 ):
     z, y, x, c = place()
     kv = NY * z + y
@@ -348,8 +348,10 @@
         both = res[two(pair)].reshape(128, 512).astype(F32)
         fed = (both * mlp_gain[...].astype(F32).reshape(1, 512)).astype(BF16)
         part = jnp.dot(fed, wu[...], preferred_element_type=F32).astype(BF16)
-        upb[two(pair)] = part.reshape(2, 64, 512)
-        send(upb.at[2 * pair + 1 - c], dd.at[pair], dd_s, dd_r.at[pair], {"c": 1 - c})
+        upb[two(pair)] = part.reshape(2, NX, 16, 512)
+        for device in tps:
+            src = upb.at[2 * pair + device["c"], device["x"]]
+            send(src, ur.at[pair, tp], us_s, us_r.at[pair], device)
 
     def squares():
         own = res[z, rows, :].astype(F32)
@@ -357,19 +359,10 @@
         for device in tps:
             send(sq2.at[tp], sq2.at[tp], sq2_s, sq2_r, device)
 
-    def across(pair):
-        wait(dd.at[pair], dd_r.at[pair])
-        total = upb[2 * pair + c].astype(F32) + dd[pair].astype(F32)
-        us[pair] = total.astype(BF16).reshape(NX, 16, 512)
-        for dx in (2, 1, 3):
-            xs = around(x, dx, NX)
-            send(us.at[pair, xs], ur.at[pair, x], us_s, us_r.at[pair], {"x": xs})
-
     def activate(pair):
-        wait(ur.at[pair, pl.ds(0, 3)], us_r.at[pair])
-        total = us[pair, x].astype(F32)
-        for dx in (1, 3, 2):
-            total = total + ur[pair, around(x, dx, NX)].astype(F32)
+        ur[pair, tp] = upb[2 * pair + c, x]
+        wait(ur.at[pair, pl.ds(0, 7)], us_r.at[pair])
+        total = jnp.sum(ur[pair].astype(F32), axis=0)
         act[2 * pair + c, x] = jnp.square(jnp.maximum(total, 0.0)).astype(BF16)
         piece = act.at[2 * pair + c, x]
         for dx in (2, 1, 3):
@@ -401,9 +394,9 @@
                 send(zs.at[j], zr.at[z], zr_s, zr_r, {"z": j})
 
     stages = (
-        (0.0, relay), (2.0, raise_up), (3.1, across), (5.2, activate), (7.3, hand_over), (8.4, bring_down), (10.5, settle),
+        (0.0, relay), (2.0, raise_up), (5.2, activate), (7.3, hand_over), (8.4, bring_down), (10.5, settle),
     )
-    gaps = [(5, 1), (5, 2), (6, 2), (6, 3)]
+    gaps = [(4, 1), (4, 2), (5, 2), (5, 3)]
     order = sorted((offset + turn, stage, turn) for stage, (offset, _) in enumerate(stages) for turn in range(4))
     pltpu.make_async_copy(wu_hbm, wu, in_sem.at[1]).wait()
     pltpu.make_async_copy(wdn_hbm, wdn, in_sem.at[2]).wait()
@@ -451,11 +444,39 @@
     wait(op.at[pl.ds(0, 7)], rz_s)
     wait(res.at[:, :, slice(0, 384)], ry_s)
     wait(sq2.at[pl.ds(0, 7)], sq2_s)
-    wait(dd, dd_s)
-    wait(us.at[pl.ds(0, 3)], us_s)
+    wait(ur.at[:, pl.ds(0, 7)], us_s)
     wait(act.at[pl.ds(0, 7)], ac_s)
     wait(dyb.at[pl.ds(0, 3)], dy_s)
     wait(zr.at[pl.ds(0, 7)], zr_s)
+
+
+PARTS = 8
+
+
+def flush_kernel(out, state, out_hbm, state_hbm, sem):
+    wide = state.shape[1] // PARTS
+    copies = [pltpu.make_async_copy(out, out_hbm, sem.at[PARTS])]
+    for number in range(PARTS):
+        part = pl.ds(number * wide, wide)
+        copies.append(pltpu.make_async_copy(state.at[:, part], state_hbm.at[:, part], sem.at[number]))
+    for copy in copies:
+        copy.start()
+    for copy in copies:
+        copy.wait()
+
+
+def flush(out, state):
+    vmem = pl.BlockSpec(memory_space=pltpu.VMEM)
+    hbm = pl.BlockSpec(memory_space=pltpu.HBM)
+    return pl.pallas_call(
+        flush_kernel,
+        out_shape=(jax.ShapeDtypeStruct(out.shape, out.dtype), jax.ShapeDtypeStruct(state.shape, state.dtype)),
+        in_specs=[vmem, vmem],
+        out_specs=(hbm, hbm),
+        scratch_shapes=[pltpu.SemaphoreType.DMA((PARTS + 1,))],
+        compiler_params=pltpu.CompilerParams(vmem_limit_bytes=1 << 20),
+        name="flush",
+    )(out, state)
 
 
 def body(
@@ -464,7 +485,7 @@
 ):
     dma = pltpu.SemaphoreType.DMA
     vmem = pl.BlockSpec(memory_space=pltpu.VMEM)
-    return pl.pallas_call(
+    out, state = pl.pallas_call(
         layer_kernel,
         out_shape=(pltpu.VMEM((16, 512), BF16), pltpu.VMEM((16, 65536), F32)),
         in_specs=[pl.BlockSpec(memory_space=pltpu.HBM)] * 14,
@@ -496,10 +517,8 @@
             pltpu.VMEM((8, 64, 128), BF16),
             pltpu.VMEM((NZ, 64, 512), BF16),
             pltpu.VMEM((8, 16, 128), F32),
-            pltpu.VMEM((8, 64, 512), BF16),
-            pltpu.VMEM((4, 64, 512), BF16),
-            pltpu.VMEM((4, NX, 16, 512), BF16),
-            pltpu.VMEM((4, NX, 16, 512), BF16),
+            pltpu.VMEM((8, NX, 16, 512), BF16),
+            pltpu.VMEM((4, 8, 16, 512), BF16),
             pltpu.VMEM((8, NX, 16, 512), BF16),
             pltpu.VMEM((8, NY, 16, 512), BF16),
             pltpu.VMEM((NY, 8, 16, 512), BF16),
@@ -508,7 +527,7 @@
             dma((9,)), dma, dma((NX,)), dma, dma, dma((8,)), dma((NZ,)), dma, dma((32,)), dma((NZ,)),
             dma((5,)), dma, dma((14,)), dma((2, NZ)), dma, dma((NY,)), dma, dma((3,)),
             dma, dma, dma, dma, dma, dma, dma, dma((NZ,)), dma, dma((32,)), dma, dma,
-            dma, dma((4,)), dma, dma((4,)), dma, dma((4,)), dma((4,)), dma, dma((4,)), dma, dma,
+            dma, dma((4,)), dma, dma((4,)), dma((4,)), dma, dma((4,)), dma, dma,
         ],
         compiler_params=pltpu.CompilerParams(collective_id=0, has_side_effects=True, vmem_limit_bytes=(59 << 20) + (800 << 10)),
         name="layer",
@@ -516,6 +535,7 @@
         hidden_rows, norm_gain, decay_bias, head_gain, mlp_gain, w_query, w_key, w_decay, w_value, w_gate,
         w_out, w_up, w_down, carried_state,
     )
+    return flush(out, state)
 
 
 def solution(mesh):

time: 79.1 us -> 78.4 us (level); the launches traced: 78.9 us -> 77.2 us
  local copies, waits for them, and re-layouts: 2.62 us -> 0 us
  Pallas kernels: 75.6 us -> 76.6 us
    unnamed x2 -> x0, local copies, waits for them, and re-layouts: 2.62 us -> none
    pallas_call x0 -> x1, Pallas kernels: none -> 2.09 us  [flush(): pl.pallas_call(flush_kernel, out_shape=(jax.ShapeDtypeStruct(out.shape, o...]
    pallas_call x1, Pallas kernels: 75.6 us -> 74.5 us  [body(): pl.pallas_call(layer_kernel, out_shape=(pltpu.VMEM((16, 512), BF16), pltp...]
where the time goes in v6:
time: 78.4 us; the launch traced here: 77.2 us
  Pallas kernels  76.6 us (98%)
    pallas_call x1, Pallas kernels, body(): pl.pallas_call(layer_kernel, out_shape=(pltpu.VMEM((16, 512), BF16), pltp...  74.5 us
    pallas_call x1, Pallas kernels, flush(): pl.pallas_call(flush_kernel, out_shape=(jax.ShapeDtypeStruct(out.shape, o...  2.09 us

profile of v6, /device:TPU:2, one launch (start us, length us, event | category | flops | bytes accessed | tf_op | source)
XLA Modules:
  0.0 77.2 jit_solution(7068026339451264899)
XLA Ops:
  0.6 74.5 %layer.1 = (bf16[16,512]{1,0:T(8,128)(2,1)S(1)}, f32[16,65536]{1,0:T(8,128)S(1)}) custom-call(bf16[16,512]{1,0:T(8,128)(2,1)} %hid_hbm.1, bf16[4096]{0:T(1024)(128)(2,1)} %norm_gain_hbm.1, f32[256]{0:T(256)} %bias_hbm.1, bf16[256]{0:T(256)(128)(2,1)} %head_gain_hbm.1, bf16[512]{0:T(512)(128)(2,1)} %mlp_gain_hbm.1, bf16[128,256]{1,0:T(8,128)(2,1)} %wq.1, ...), custom_call_target="tpu_custom_call" | custom-call | tf_op jit(solution)/shard_map/layer/pallas_call | solution.py:488
  75.1 2.1 %flush.1 = (bf16[16,512]{1,0:T(8,128)(2,1)}, f32[16,65536]{1,0:T(8,128)}) custom-call(bf16[16,512]{1,0:T(8,128)(2,1)S(1)} %get-tuple-element.4.out, f32[16,65536]{1,0:T(8,128)S(1)} %get-tuple-element.5.state), custom_call_target="tpu_custom_call" | custom-call | tf_op jit(solution)/shard_map/flush/pallas_call | solution.py:471

commit v7 on v6

--- a/solution.py
+++ b/solution.py
@@ -226,10 +226,10 @@
     spread_c(GROUPS[0])
     pass_on(3, 0)
     spread_c(GROUPS[1])
-    pass_on(3, 1)
     by_width(lambda width: wait(wb.at[:, :, slice(0, width)], wb_r))
     multiply(GROUPS[0])
     spread_c(GROUPS[2])
+    pass_on(3, 1)
     by_width(lambda width: scatter(0, 0, width))
     multiply(GROUPS[1])
     spread_c(GROUPS[3])

time: 78.4 us -> 78.3 us (level)
  no operation moved by 1% of the time
where the time goes in v7:
time: 78.3 us; the launch traced here: 77.1 us
  Pallas kernels  76.5 us (98%)
    pallas_call x1, Pallas kernels, body(): pl.pallas_call(layer_kernel, out_shape=(pltpu.VMEM((16, 512), BF16), pltp...  74.4 us
    pallas_call x1, Pallas kernels, flush(): pl.pallas_call(flush_kernel, out_shape=(jax.ShapeDtypeStruct(out.shape, o...  2.09 us

profile of v7, /device:TPU:2, one launch (start us, length us, event | category | flops | bytes accessed | tf_op | source)
XLA Modules:
  0.0 77.1 jit_solution(17404223189609081343)
XLA Ops:
  0.6 74.4 %layer.1 = (bf16[16,512]{1,0:T(8,128)(2,1)S(1)}, f32[16,65536]{1,0:T(8,128)S(1)}) custom-call(bf16[16,512]{1,0:T(8,128)(2,1)} %hid_hbm.1, bf16[4096]{0:T(1024)(128)(2,1)} %norm_gain_hbm.1, f32[256]{0:T(256)} %bias_hbm.1, bf16[256]{0:T(256)(128)(2,1)} %head_gain_hbm.1, bf16[512]{0:T(512)(128)(2,1)} %mlp_gain_hbm.1, bf16[128,256]{1,0:T(8,128)(2,1)} %wq.1, ...), custom_call_target="tpu_custom_call" | custom-call | tf_op jit(solution)/shard_map/layer/pallas_call | solution.py:488
  75.0 2.1 %flush.1 = (bf16[16,512]{1,0:T(8,128)(2,1)}, f32[16,65536]{1,0:T(8,128)}) custom-call(bf16[16,512]{1,0:T(8,128)(2,1)S(1)} %get-tuple-element.4.out, f32[16,65536]{1,0:T(8,128)S(1)} %get-tuple-element.5.state), custom_call_target="tpu_custom_call" | custom-call | tf_op jit(solution)/shard_map/flush/pallas_call | solution.py:471
